TPU v7x, 32 devices: a whole 2x2x4 slice. The times are simulated.
32 devices in a mesh: sp: 8 (over z, core), tp: 4 (over y, x).
Axes of the slice: x: 2, y: 2, z: 4, core: 2. Of those that a mesh axis runs over, the one named last changes fastest.
Arguments:
- query_pairs: bfloat16 [2048, 2048], P('sp', 'tp'), may hold values from -8 to 8
- key_pairs: bfloat16 [2048, 2048], P('sp', 'tp'), may hold values from -6 to 6
- value_rows: bfloat16 [2048, 2048], P('sp', 'tp'), may hold values from -6 to 6
- doc_ids: int32 [2048], P('sp'), may hold values from 0 to 3, never falling along the last dimension, each value on 1 to 1280 neighbouring positions
- contrast_lambda: float32 [32], P('tp'), may hold values from 0.3 to 0.8
- head_gain: float32 [64], replicated, may hold values from 0.1 to 1.9
- stream: bfloat16 [2048, 2048], P('sp', 'tp'), may hold values from -6 to 6
- out_proj: bfloat16 [2048, 2048], P(None, 'tp'), may hold values from -0.125 to 0.125
- norm_gain: float32 [2048], replicated, may hold values from 0.1 to 1.9
- routes: int32 [2048, 2], P('sp'), may hold values from 0 to 7, all different within a row; in each aligned block of 256 rows (0 to 255, 256 to 511, ...) at most 128 rows name the same one
- route_weights: float32 [2048, 2], P('sp'), may hold values from 0.3 to 1.5
- expert_gate: bfloat16 [8, 2048, 2048], P('sp', None, 'tp'), may hold values from -0.125 to 0.125
- expert_up: bfloat16 [8, 2048, 2048], P('sp', None, 'tp'), may hold values from -0.125 to 0.125
- expert_down: bfloat16 [8, 2048, 2048], P('sp', None, 'tp'), may hold values from -0.125 to 0.125
- shared_gate: bfloat16 [2048, 2048], P(None, 'tp'), may hold values from -0.125 to 0.125
- shared_up: bfloat16 [2048, 2048], P(None, 'tp'), may hold values from -0.125 to 0.125
- shared_down: bfloat16 [2048, 2048], P(None, 'tp'), may hold values from -0.125 to 0.125
Outputs:
- mixed: bfloat16 [2048, 2048], P('sp', 'tp')
Inputs may be any that keep to these rules, and one draw needn't show every extreme that they name: `doc_ids`: document numbers never fall along the positions; a document holds at most 1280 positions. `routes`: A position names 2 different experts. In each aligned block of 256 rows no expert is named by more than 128 rows, and every draw has a block in which some expert is named by exactly 128 rows.
All inputs are finite; a program needn't handle non-finite values.
Results may differ from a plain program's by a relative error of at most 0.011.
Values may be sent and summed in bfloat16 or wider, within the bound.
A program may use at most 64 MiB of HBM per device.

v0:
```python
import functools
import math

import jax
import jax.numpy as jnp
from jax import lax
from jax.experimental import pallas as pl
from jax.experimental.pallas import tpu as pltpu
from jax.sharding import PartitionSpec as P

epsilon = 1e-06
floor_score = -1e30


def add_columns(weight_rows, part_block):
    return jnp.dot(part_block, weight_rows, preferred_element_type=jnp.float32)


def shards(
    query_pairs,
    key_pairs,
    value_rows,
    doc_ids,
    contrast_lambda,
    head_gain,
    stream,
    out_proj,
    norm_gain,
    routes,
    route_weights,
    expert_gate,
    expert_up,
    expert_down,
    shared_gate,
    shared_up,
    shared_down,
):
    row_count = query_pairs.shape[0]
    local_heads = contrast_lambda.shape[0]
    key_width = query_pairs.shape[1] // (2 * local_heads)
    value_width = value_rows.shape[1] // local_heads
    scaling = key_width ** (-0.5)
    first_row = lax.axis_index("sp") * row_count
    query_pos = first_row + jnp.arange(row_count, dtype=jnp.int32)
    last_query = first_row + row_count - 1
    first_doc = doc_ids[0]
    query_split = query_pairs.reshape(row_count, local_heads, 2, key_width)

    def absorb_block(running, key_block, value_block, doc_block, key_start):
        best, denom, numer = running
        span_len = key_block.shape[0]
        key_pos = key_start + jnp.arange(span_len, dtype=jnp.int32)
        allowed = (key_pos[None, :] <= query_pos[:, None]) & (
            doc_block[None, :] == doc_ids[:, None]
        )
        scores = (
            jnp.einsum(
                "qhmd,khmd->hmqk",
                query_split,
                key_block.reshape(span_len, local_heads, 2, key_width),
                preferred_element_type=jnp.float32,
            )
            * scaling
        )
        scores = jnp.where(allowed, scores, floor_score)
        new_best = jnp.maximum(best, jnp.max(scores, axis=-1))
        weights = jnp.where(allowed, jnp.exp(scores - new_best[..., None]), 0.0)
        fade = jnp.exp(best - new_best)
        denom = denom * fade + jnp.sum(weights, axis=-1)
        numer = numer * fade[..., None] + jnp.einsum(
            "hmqk,khv->hmqv",
            weights.astype(jnp.bfloat16),
            value_block.reshape(span_len, local_heads, value_width),
            preferred_element_type=jnp.float32,
        )
        return (new_best, denom, numer)

    start_best = jnp.full((local_heads, 2, row_count), floor_score, jnp.float32)
    start_denom = jnp.zeros((local_heads, 2, row_count), jnp.float32)
    start_numer = jnp.zeros((local_heads, 2, row_count, value_width), jnp.float32)
    key_piece = lax.all_gather(key_pairs, "sp", axis=0, tiled=True)
    value_piece = lax.all_gather(value_rows, "sp", axis=0, tiled=True)
    doc_piece = lax.all_gather(doc_ids, "sp", axis=0, tiled=True)
    length = key_piece.shape[0]
    span_len = row_count * max(1, 512 // row_count)

    def one_span(span_index, carried):
        offset = span_index * span_len
        key_block = lax.dynamic_slice_in_dim(key_piece, offset, span_len, 0)
        value_block = lax.dynamic_slice_in_dim(value_piece, offset, span_len, 0)
        doc_block = lax.dynamic_slice_in_dim(doc_piece, offset, span_len, 0)
        needed = (offset <= last_query) & (doc_block[span_len - 1] >= first_doc)
        return lax.cond(
            needed,
            lambda held: absorb_block(held, key_block, value_block, doc_block, offset),
            lambda held: held,
            carried,
        )

    best, denom, numer = lax.fori_loop(
        0, length // span_len, one_span, (start_best, start_denom, start_numer)
    )
    heard = numer / denom[..., None]
    contrast = heard[:, 0] - contrast_lambda[:, None, None] * heard[:, 1]
    contrast = (
        contrast
        * lax.rsqrt(jnp.mean(contrast * contrast, axis=-1, keepdims=True) + epsilon)
        * head_gain
    )
    head_out = (
        jnp.transpose(contrast, (1, 0, 2))
        .reshape(row_count, local_heads * value_width)
        .astype(jnp.bfloat16)
    )
    projected = add_columns(out_proj, lax.all_gather(head_out, "tp", axis=1, tiled=True))
    hidden_cols = (stream.astype(jnp.float32) + projected).astype(jnp.bfloat16)
    hidden_rows = lax.all_gather(hidden_cols, "tp", axis=1, tiled=True)
    widened = hidden_rows.astype(jnp.float32)
    normed = (
        widened
        * lax.rsqrt(jnp.mean(widened * widened, axis=-1, keepdims=True) + epsilon)
        * norm_gain
    ).astype(jnp.bfloat16)
    shared_act = (
        jax.nn.silu(jnp.dot(normed, shared_gate, preferred_element_type=jnp.float32))
        * jnp.dot(normed, shared_up, preferred_element_type=jnp.float32)
    ).astype(jnp.bfloat16)
    shared_cols = add_columns(shared_down, lax.all_gather(shared_act, "tp", axis=1, tiled=True))
    expert_count = lax.axis_size("sp")
    route_count = routes.shape[1]
    capacity = 2 * row_count * route_count // expert_count
    flat_routes = routes.reshape(-1)
    hits = (flat_routes[:, None] == jnp.arange(expert_count, dtype=jnp.int32)[None, :]).astype(
        jnp.int32
    )
    position = jnp.sum(jnp.cumsum(hits, axis=0) * hits, axis=1) - 1
    target = flat_routes * capacity + position
    sources = jnp.arange(flat_routes.shape[0], dtype=jnp.int32) // route_count
    owner = jnp.zeros((expert_count * capacity,), jnp.int32).at[target].set(sources)
    outgoing = normed[owner].reshape(expert_count, capacity, normed.shape[1])
    gate_cols = expert_gate[0]
    up_cols = expert_up[0]
    down_cols = expert_down[0]
    slice_width = outgoing.shape[2] // lax.axis_size("tp")
    own_slice = lax.dynamic_slice_in_dim(
        outgoing, lax.axis_index("tp") * slice_width, slice_width, 2
    )
    arrived = lax.all_to_all(own_slice, "sp", split_axis=0, concat_axis=0, tiled=True)
    apply_arrived = lax.all_gather(arrived, "tp", axis=2, tiled=True)
    gated = jnp.einsum("snd,df->snf", apply_arrived, gate_cols, preferred_element_type=jnp.float32)
    lifted = jnp.einsum("snd,df->snf", apply_arrived, up_cols, preferred_element_type=jnp.float32)
    expert_act = (jax.nn.silu(gated) * lifted).astype(jnp.bfloat16)
    expert_out = add_columns(
        down_cols, lax.all_gather(expert_act, "tp", axis=2, tiled=True)
    ).astype(jnp.bfloat16)
    returned = lax.all_to_all(expert_out, "sp", split_axis=0, concat_axis=0, tiled=True)
    flat_back = returned.reshape(expert_count * capacity, returned.shape[2])
    picked = (
        flat_back[target].reshape(row_count, route_count, returned.shape[2]).astype(jnp.float32)
    )
    routed = jnp.sum(picked * route_weights[:, :, None], axis=1)
    return (hidden_cols.astype(jnp.float32) + shared_cols + routed).astype(jnp.bfloat16)


MESH_ID = pl.DeviceIdType.MESH
VMEM = pl.BlockSpec(memory_space=pltpu.VMEM)
ANY = pl.BlockSpec(memory_space=pl.ANY)
SMEM = pl.BlockSpec(memory_space=pltpu.SMEM)


def flip(index, mask, size):
    out, bit = 0, 1
    while bit < size:
        out = out + bit * lax.rem(lax.div(index, bit) + lax.div(mask, bit), 2)
        bit *= 2
    return out


def remote(src, dst, send, recv, device):
    return pltpu.make_async_remote_copy(
        src_ref=src,
        dst_ref=dst,
        send_sem=send,
        recv_sem=recv,
        device_id=device,
        device_id_type=MESH_ID,
    )


def greet(devices):
    barrier = pltpu.get_barrier_semaphore()
    for device in devices:
        pl.semaphore_signal(barrier, inc=1, device_id=device, device_id_type=MESH_ID)
    pl.semaphore_wait(barrier, len(devices))


def spread_kernel(
    count, width, q_ref, k_ref, v_ref, doc_ref, out_ref, docs_ref, pack, send, recv, dsend, drecv
):
    me, col = lax.axis_index("sp"), lax.axis_index("tp")
    rows = q_ref.shape[0]
    half = rows // 2
    peers = [(flip(me, jnp.int32(k), count), col) for k in range(count)]
    for h in range(count):
        cut = slice(h * width, (h + 1) * width)
        pack[h, :rows, :] = jnp.concatenate([q_ref[:, cut], k_ref[:, cut]], axis=1)
        pack[h, rows:, :] = jnp.concatenate([v_ref[:half, cut], v_ref[half:, cut]], axis=1)
    greet(peers[1:])
    copies = []
    for k in reversed(range(1, count)):
        there = peers[k]
        copies.append(remote(doc_ref, docs_ref.at[me], dsend.at[k], drecv.at[k], there))
        copies.append(remote(pack.at[there[0]], out_ref.at[me], send.at[k], recv.at[k], there))
        copies[-2].start()
        copies[-1].start()
    out_ref[me] = pack[me]
    docs_ref[me] = doc_ref[...]
    for copy in copies:
        copy.wait()


def attend_kernel(
    scaling, lam_ref, qkv_ref, doc_ref, gain_ref, out_ref, turned
):
    count, rows = doc_ref.shape[0], doc_ref.shape[2]
    half = rows // 2
    width = gain_ref.shape[1]
    weight = lam_ref[lax.axis_index("sp")]
    gains = jnp.concatenate([gain_ref[...], gain_ref[...]], axis=1)
    doc_rows = jnp.concatenate([doc_ref[b] for b in range(count)], axis=0).astype(jnp.float32)
    doc_cols = jnp.transpose(doc_rows)
    key_width = width // 2
    lanes = lax.broadcasted_iota(jnp.int32, (rows, 2 * width), 1)
    factor = scaling * math.log2(math.e)

    @pl.loop(0, count)
    def _(b):
        turned[b] = jnp.transpose(qkv_ref[b, rows:, :].astype(jnp.float32)).astype(jnp.bfloat16)

    @pl.loop(0, count)
    def _(b):
        moved = pltpu.roll(qkv_ref[b, :rows, :].astype(jnp.float32), width, 1)
        queries = [
            jnp.where(
                (lanes >= width + m * key_width) & (lanes < width + (m + 1) * key_width),
                moved,
                0.0,
            ).astype(jnp.bfloat16)
            for m in range(2)
        ]
        own_docs = doc_ref[b].astype(jnp.float32)
        earlier = jnp.zeros((rows, rows), jnp.float32)
        for kb in range(count):
            earlier = earlier + jnp.where(doc_cols[:, kb : kb + 1] < own_docs, 1.0, 0.0)
        earlier = jnp.sum(earlier, axis=0, keepdims=True)
        starts = earlier.astype(jnp.int32)
        first = lax.div(jnp.min(earlier).astype(jnp.int32), rows)
        query_pos = b * rows + lax.broadcasted_iota(jnp.int32, (1, rows), 1)

        def step(i, carried):
            tiles = []
            for part in range(2):
                kb = b - 2 * i - part
                key_pos = kb * rows + lax.broadcasted_iota(jnp.int32, (rows, rows), 0)
                allowed = (key_pos <= query_pos) & (key_pos >= starts)
                tiles.append((jnp.maximum(kb, 0), allowed))
            scores = [
                [
                    jnp.where(
                        allowed,
                        lax.dot_general(
                            qkv_ref[kb, :rows, :], queries[m], (((1,), (1,)), ((), ())),
                            preferred_element_type=jnp.float32,
                        )
                        * factor,
                        floor_score,
                    )
                    for kb, allowed in tiles
                ]
                for m in range(2)
            ]
            out = []
            for m in range(2):
                best, denom, numer = carried[m]
                tallest = jnp.max(jnp.maximum(*scores[m]), axis=0, keepdims=True)
                new_best = jnp.maximum(best, tallest)
                fade = jnp.exp2(best - new_best)
                weights = [jnp.exp2(tile - new_best) for tile in scores[m]]
                denom = denom * fade + jnp.sum(weights[0] + weights[1], axis=0, keepdims=True)
                numer = numer * fade
                for (kb, _), tile in zip(tiles, weights):
                    rounded = tile.astype(jnp.bfloat16)
                    numer = (
                        numer
                        + jnp.dot(
                            turned[kb, :width, :], rounded[:half],
                            preferred_element_type=jnp.float32,
                        )
                        + jnp.dot(
                            turned[kb, width:, :], rounded[half:],
                            preferred_element_type=jnp.float32,
                        )
                    )
                out.append((new_best, denom, numer))
            return tuple(out)

        begin = tuple(
            (
                jnp.full((1, rows), floor_score, jnp.float32),
                jnp.zeros((1, rows), jnp.float32),
                jnp.zeros((width, rows), jnp.float32),
            )
            for _ in range(2)
        )
        done = lax.fori_loop(0, lax.div(b - first, 2) + 1, step, begin)
        heard = [numer / denom for _, denom, numer in done]
        contrast = heard[0] - weight * heard[1]
        contrast = contrast * lax.rsqrt(
            jnp.mean(contrast * contrast, axis=0, keepdims=True) + epsilon
        )
        stacked = jnp.concatenate([contrast[:, :half], contrast[:, half:]], axis=0)
        out_ref[b] = (jnp.transpose(stacked) * gains).astype(jnp.bfloat16)


def layer_kernel(
    count,
    capacity,
    heads_ref,
    stream_ref,
    gain_ref,
    routes_ref,
    weight_ref,
    proj_hbm,
    sgate_hbm,
    sup_hbm,
    sdown_hbm,
    gate_hbm,
    up_hbm,
    down_hbm,
    out_ref,
    proj,
    sgate,
    sup,
    sdown,
    gate,
    up,
    down,
    held,
    head_buf,
    hidden_buf,
    normed,
    shared_buf,
    onehot,
    outgoing,
    rows_in,
    acts,
    made,
    back,
    shared_cols,
    load_sem,
    hsend,
    hrecv,
    gsend,
    grecv,
    zsend,
    zrecv,
    rsend,
    rrecv,
):
    me, col = lax.axis_index("sp"), lax.axis_index("tp")
    rows, cols = stream_ref.shape
    half = rows // 2
    width = heads_ref.shape[2] // 2
    f32 = jnp.float32
    loads = [
        pltpu.make_async_copy(a, b, load_sem.at[i])
        for i, (a, b) in enumerate(
            (
                (proj_hbm, proj),
                (sgate_hbm, sgate),
                (sup_hbm, sup),
                (gate_hbm, gate),
                (up_hbm, up),
                (sdown_hbm, sdown),
                (down_hbm, down),
            )
        )
    ]
    for load in loads:
        load.start()
    side = [flip(col, jnp.int32(j), 4) for j in range(4)]
    peer = lambda k: (flip(me, k, count), col)
    near_x, near_y = (me, side[1]), (me, side[2])
    greet([peer(jnp.int32(k)) for k in range(1, count)] + [near_x, near_y])

    def direct(buf, row, index):
        own = buf.at[(0,) + index]
        return (
            remote(own, buf.at[(1,) + index], gsend.at[row, 0], grecv.at[row, 0], near_x),
            remote(own, buf.at[(2,) + index], gsend.at[row, 1], grecv.at[row, 1], near_y),
        )

    def relays(buf, row, index):
        middle = buf.shape[-2] // 2
        top, low = pl.ds(0, middle), pl.ds(middle, middle)
        return (
            remote(
                buf.at[(1,) + index + (top,)], buf.at[(3,) + index + (top,)],
                gsend.at[row, 2], grecv.at[row, 2], near_y,
            ),
            remote(
                buf.at[(2,) + index + (low,)], buf.at[(3,) + index + (low,)],
                gsend.at[row, 3], grecv.at[row, 3], near_x,
            ),
        )

    def offer(buf, row, index=()):
        for copy in direct(buf, row, index):
            copy.start()

    def pass_on(buf, row, index=()):
        for first, second in zip(direct(buf, row, index), relays(buf, row, index)):
            first.wait_recv()
            second.start()

    def finish(buf, row, index=()):
        for copy in relays(buf, row, index):
            copy.wait_recv()

    def drain(buf, row, index=()):
        for copy in direct(buf, row, index) + relays(buf, row, index):
            copy.wait_send()

    row_head, row_hidden, row_shared = 2 * count, 2 * count + 2, 2 * count + 4

    head_copies = []
    for k in reversed(range(1, count)):
        there = peer(jnp.int32(k))
        head_copies.append(
            remote(heads_ref.at[there[0]], held.at[me], hsend.at[k], hrecv.at[k], there)
        )
        head_copies[-1].start()
    held[me] = heads_ref[me]

    near = routes_ref[...] ^ me
    lane = lax.broadcasted_iota(jnp.int32, (128, rows), 0)
    hits = [near[j : j + 1, :] == lane for j in range(2)]
    present = hits[0] | hits[1]
    before = (
        lax.broadcasted_iota(jnp.int32, (rows, rows), 0)
        < lax.broadcasted_iota(jnp.int32, (rows, rows), 1)
    )
    place = jnp.dot(
        present.astype(f32).astype(jnp.bfloat16),
        before.astype(f32).astype(jnp.bfloat16),
        preferred_element_type=f32,
    )
    place = jnp.where(present, place, -1.0)
    slot = lax.broadcasted_iota(jnp.int32, (capacity, rows), 0).astype(f32)
    for k in range(count):
        onehot[k] = (slot == place[k : k + 1, :]).astype(f32).astype(jnp.bfloat16)
    portion = jnp.where(hits[0], weight_ref[0:1, :], 0.0) + jnp.where(
        hits[1], weight_ref[1:2, :], 0.0
    )
    portions = jnp.transpose(portion)

    for copy in head_copies:
        copy.wait_recv()
    for pair in range(count // 2):
        first, second = held[2 * pair], held[2 * pair + 1]
        cut = slice(2 * pair * width, 2 * (pair + 1) * width)
        for h in range(2):
            part = slice(h * width, (h + 1) * width)
            head_buf[0, h, :, cut] = jnp.concatenate([first[:, part], second[:, part]], axis=1)
    for h in range(2):
        offer(head_buf, row_head + h, (h,))
    loads[0].wait()
    totals = [jnp.dot(head_buf[0, h], proj[col], preferred_element_type=f32) for h in range(2)]
    for h in range(2):
        pass_on(head_buf, row_head + h, (h,))
    for h in range(2):
        total = totals[h]
        for j in (1, 2):
            total = total + jnp.dot(head_buf[j, h], proj[side[j]], preferred_element_type=f32)
        finish(head_buf, row_head + h, (h,))
        total = total + jnp.dot(head_buf[3, h], proj[side[3]], preferred_element_type=f32)
        span = slice(h * half, (h + 1) * half)
        hidden_buf[0, h] = (stream_ref[span, :].astype(f32) + total).astype(jnp.bfloat16)
        offer(hidden_buf, row_hidden + h, (h,))
    for h in range(2):
        pass_on(hidden_buf, row_hidden + h, (h,))
    for h in range(2):
        finish(hidden_buf, row_hidden + h, (h,))
        squares = jnp.zeros((half, cols), f32)
        for j in range(4):
            wide = hidden_buf[j, h].astype(f32)
            squares = squares + wide * wide
        mean = jnp.sum(squares, axis=1, keepdims=True) / (4 * cols)
        scale = lax.rsqrt(mean + epsilon)
        span = slice(h * half, (h + 1) * half)
        for j in range(4):
            wide = hidden_buf[j, h].astype(f32)
            normed[j, span, :] = (wide * scale * gain_ref[side[j]]).astype(jnp.bfloat16)

    def dispatch_far(k):
        return remote(outgoing.at[0, k], rows_in.at[0, k], zsend.at[k], zrecv.at[k], peer(k))

    def dispatch_near(k):
        return remote(outgoing.at[:, k], rows_in.at[:, k], zsend.at[k], zrecv.at[k], peer(k))

    def chosen(k, j):
        return jnp.dot(onehot[k], normed[j], preferred_element_type=f32).astype(jnp.bfloat16)

    for k in range(4, count):
        outgoing[0, k] = chosen(k, 0)
        dispatch_far(jnp.int32(k)).start()
    for j in range(4):
        outgoing[j, 1] = chosen(1, j)
    dispatch_near(jnp.int32(1)).start()
    for j in range(4):
        rows_in[j, 0] = chosen(0, j)
    for load in loads[1:]:
        load.wait()

    def give_back(k):
        return remote(made.at[k], back.at[k], rsend.at[k], rrecv.at[k], peer(k))

    def turn(p):
        later = jnp.where(p < count - 2, p + 2, p - count + 4)
        return jnp.where(p < 2, p, later)

    @pl.loop(0, count + 2)
    def _(i):
        @pl.when((i >= 2) & (i < count - 2))
        def _():
            finish(rows_in, i + 2, (i + 2,))

        @pl.when((i == 1) | ((i >= count - 2) & (i < count)))
        def _():
            dispatch_near(turn(i)).wait_recv()

        @pl.when(i < count)
        def _():
            k = turn(i)
            gated = jnp.zeros((capacity, cols), f32)
            lifted = jnp.zeros((capacity, cols), f32)
            for j in range(4):
                gated = gated + jnp.dot(rows_in[j, k], gate[side[j]], preferred_element_type=f32)
                lifted = lifted + jnp.dot(rows_in[j, k], up[side[j]], preferred_element_type=f32)
            acts[0, k] = (jax.nn.silu(gated) * lifted).astype(jnp.bfloat16)
            offer(acts, count + k, (k,))

        @pl.when(i == 0)
        def _():
            for k in (2, 3):
                for j in range(4):
                    outgoing[j, k] = chosen(k, j)
                dispatch_near(jnp.int32(k)).start()
            gated = jnp.zeros((rows, cols), f32)
            lifted = jnp.zeros((rows, cols), f32)
            for j in range(4):
                gated = gated + jnp.dot(normed[j], sgate[side[j]], preferred_element_type=f32)
                lifted = lifted + jnp.dot(normed[j], sup[side[j]], preferred_element_type=f32)
            shared_buf[0] = (jax.nn.silu(gated) * lifted).astype(jnp.bfloat16)
            offer(shared_buf, row_shared)

        @pl.when(i < count - 4)
        def _():
            dispatch_far(i + 4).wait_recv()
            offer(rows_in, i + 4, (i + 4,))

        @pl.when((i >= 1) & (i < count + 1))
        def _():
            k = turn(i - 1)
            pass_on(acts, count + k, (k,))

        @pl.when((i >= 1) & (i < count - 3))
        def _():
            pass_on(rows_in, i + 3, (i + 3,))

        @pl.when(i == 1)
        def _():
            pass_on(shared_buf, row_shared)

        @pl.when(i == 4)
        def _():
            finish(shared_buf, row_shared)
            cols_sum = jnp.zeros((rows, cols), f32)
            for j in range(4):
                cols_sum = cols_sum + jnp.dot(
                    shared_buf[j], sdown[side[j]], preferred_element_type=f32
                )
            shared_cols[...] = cols_sum

        @pl.when(i >= 2)
        def _():
            k = turn(i - 2)
            finish(acts, count + k, (k,))
            result = jnp.zeros((capacity, cols), f32)
            for j in range(4):
                result = result + jnp.dot(acts[j, k], down[side[j]], preferred_element_type=f32)
            made[k] = result.astype(jnp.bfloat16)

            @pl.when(k > 0)
            def _():
                give_back(k).start()

    back[0] = made[0]
    for p in range(count):
        k = p if p < 2 else (p + 2 if p < count - 2 else p - count + 4)
        if k > 0:
            give_back(jnp.int32(k)).wait_recv()
        picked = lax.dot_general(
            onehot[k], back[k], (((0,), (0,)), ((), ())), preferred_element_type=f32
        )
        shared_cols[...] = shared_cols[...] + portions[:, k : k + 1] * picked
    for h in range(2):
        span = slice(h * half, (h + 1) * half)
        out_ref[span, :] = (hidden_buf[0, h].astype(f32) + shared_cols[span, :]).astype(
            jnp.bfloat16
        )

    for copy in head_copies:
        copy.wait_send()
    for h in range(2):
        drain(head_buf, row_head + h, (h,))
        drain(hidden_buf, row_hidden + h, (h,))
    drain(shared_buf, row_shared)

    @pl.loop(4, count)
    def _(k):
        drain(rows_in, k, (k,))
        dispatch_far(k).wait_send()

    @pl.loop(1, 4)
    def _(k):
        dispatch_near(k).wait_send()

    @pl.loop(0, count)
    def _(k):
        drain(acts, count + k, (k,))

        @pl.when(k > 0)
        def _():
            give_back(k).wait_send()


def head_per_device(
    query_pairs,
    key_pairs,
    value_rows,
    doc_ids,
    contrast_lambda,
    head_gain,
    stream,
    out_proj,
    norm_gain,
    routes,
    route_weights,
    expert_gate,
    expert_up,
    expert_down,
    shared_gate,
    shared_up,
    shared_down,
):
    rows, cols = stream.shape
    count, sides = lax.axis_size("sp"), lax.axis_size("tp")
    width = value_rows.shape[1] // count
    capacity = 2 * rows * routes.shape[1] // count
    bf16, f32 = jnp.bfloat16, jnp.float32
    dma = pltpu.SemaphoreType.DMA
    qkv, docs = pl.pallas_call(
        functools.partial(spread_kernel, count, width),
        out_shape=(
            jax.ShapeDtypeStruct((count, rows + rows // 2, 2 * width), bf16),
            jax.ShapeDtypeStruct((count, 1, rows), jnp.int32),
        ),
        in_specs=[VMEM] * 4,
        out_specs=(VMEM, VMEM),
        scratch_shapes=[
            pltpu.VMEM((count, rows + rows // 2, 2 * width), bf16),
            dma((count,)),
            dma((count,)),
            dma((count,)),
            dma((count,)),
        ],
        compiler_params=pltpu.CompilerParams(collective_id=0, has_side_effects=True),
        name="spread_heads",
    )(query_pairs, key_pairs, value_rows, doc_ids.reshape(1, rows))
    heads = pl.pallas_call(
        functools.partial(attend_kernel, (width // 2) ** (-0.5)),
        out_shape=jax.ShapeDtypeStruct((count, rows // 2, 2 * width), bf16),
        in_specs=[SMEM, VMEM, VMEM, VMEM],
        out_specs=VMEM,
        scratch_shapes=[pltpu.VMEM((count, 2 * width, rows // 2), bf16)],
        name="attend",
    )(
        contrast_lambda,
        qkv,
        docs,
        head_gain.reshape(1, width),
    )
    split = lambda weight: weight.reshape(sides, weight.shape[-2] // sides, weight.shape[-1])
    weight_shape = (sides, cols, cols)
    return pl.pallas_call(
        functools.partial(layer_kernel, count, capacity),
        out_shape=jax.ShapeDtypeStruct((rows, cols), bf16),
        in_specs=[VMEM] * 5 + [ANY] * 7,
        out_specs=VMEM,
        scratch_shapes=[pltpu.VMEM(weight_shape, bf16)] * 7
        + [
            pltpu.VMEM((count, rows // 2, 2 * width), bf16),
            pltpu.VMEM((sides, 2, rows // 2, cols), bf16),
            pltpu.VMEM((sides, 2, rows // 2, cols), bf16),
            pltpu.VMEM((sides, rows, cols), bf16),
            pltpu.VMEM((sides, rows, cols), bf16),
            pltpu.VMEM((count, capacity, rows), bf16),
            pltpu.VMEM((sides, count, capacity, cols), bf16),
            pltpu.VMEM((sides, count, capacity, cols), bf16),
            pltpu.VMEM((sides, count, capacity, cols), bf16),
            pltpu.VMEM((count, capacity, cols), bf16),
            pltpu.VMEM((count, capacity, cols), bf16),
            pltpu.VMEM((rows, cols), f32),
            dma((7,)),
            dma((count,)),
            dma((count,)),
            dma((2 * count + 5, 4)),
            dma((2 * count + 5, 4)),
            dma((count,)),
            dma((count,)),
            dma((count,)),
            dma((count,)),
        ],
        compiler_params=pltpu.CompilerParams(
            collective_id=1, has_side_effects=True, vmem_limit_bytes=60 * 2**20
        ),
        name="layer",
    )(
        heads,
        stream,
        norm_gain.reshape(sides, 1, cols),
        routes.T,
        route_weights.T,
        split(out_proj),
        split(shared_gate),
        split(shared_up),
        split(shared_down),
        split(expert_gate[0]),
        split(expert_up[0]),
        split(expert_down[0]),
    )


def choose(*args):
    query_pairs, value_rows, heads, stream = args[0], args[2], args[4].shape[0], args[6]
    count, sides = lax.axis_size("sp"), lax.axis_size("tp")
    width = value_rows.shape[1] // heads
    rows, cols = stream.shape
    hidden = {args[i].shape[-1] for i in (7, 11, 12, 13, 14, 15, 16)}
    fits = (
        heads == count
        and count & (count - 1) == 0
        and 8 <= count <= 128
        and sides == 4
        and 2 * width == 128
        and query_pairs.shape[1] == value_rows.shape[1] == cols
        and hidden == {cols}
        and all(args[i].shape[-2] == sides * cols for i in (7, 11, 12, 13, 14, 15, 16))
        and rows % 256 == 0
        and (2 * rows * args[9].shape[1]) % (128 * count) == 0
        and args[9].shape[1] == 2
    )
    return (head_per_device if fits else shards)(*args)


def solution(mesh):
    return jax.shard_map(
        choose,
        mesh=mesh,
        in_specs=(
            P("sp", "tp"),
            P("sp", "tp"),
            P("sp", "tp"),
            P("sp"),
            P("tp"),
            P(),
            P("sp", "tp"),
            P(None, "tp"),
            P(),
            P("sp", None),
            P("sp", None),
            P("sp", None, "tp"),
            P("sp", None, "tp"),
            P("sp", None, "tp"),
            P(None, "tp"),
            P(None, "tp"),
            P(None, "tp"),
        ),
        out_specs=P("sp", "tp"),
        check_vma=False,
    )
```

profile of v0, /device:TPU:0, one launch (start us, length us, event | category | flops | bytes accessed | tf_op | source)
XLA Modules:
  0.0 154.2 jit_solution(13121770240315399719)
XLA Ops:
  0.0 26.1 %spread_heads.1 = (bf16[8,384,128]{2,1,0:T(8,128)(2,1)}, s32[8,1,256]{2,1,0:T(1,128)}) custom-call(bf16[256,512]{1,0:T(8,128)(2,1)} %q_ref.1, bf16[256,512]{1,0:T(8,128)(2,1)} %k_ref.1, bf16[256,512]{1,0:T(8,128)(2,1)} %v_ref.1, s32[1,256]{1,0:T(1,128)} %bitcast.22), custom_call_target="tpu_custom_call" | custom-call | tf_op jit(solution)/shard_map/spread_heads/pallas_call | solution.py:673
  26.1 17.1 %attend.1.heads_ref = bf16[8,128,128]{2,1,0:T(8,128)(2,1)} custom-call(f32[8]{0:T(128)} %lam_ref.1, bf16[8,384,128]{2,1,0:T(8,128)(2,1)} %get-tuple-element.7.qkv_ref, s32[8,1,256]{2,1,0:T(1,128)} %get-tuple-element.8.doc_ref, f32[1,64]{1,0:T(1,128)} %bitcast.23), custom_call_target="tpu_custom_call" | custom-call | tf_op jit(solution)/shard_map/attend/pallas_call | solution.py:691
  43.2 109.3 %layer.1 = bf16[256,512]{1,0:T(8,128)(2,1)} custom-call(bf16[8,128,128]{2,1,0:T(8,128)(2,1)} %attend.1.heads_ref, bf16[256,512]{1,0:T(8,128)(2,1)} %stream_ref.1, f32[4,1,512]{2,1,0:T(1,128)} %bitcast.19, s32[2,256]{1,0:T(2,128)} %bitcast.20, f32[2,256]{1,0:T(2,128)} %bitcast.21, bf16[4,512,512]{2,1,0:T(8,128)(2,1)} %bitcast.12, ...), custom_call_target="tpu_custom_call" | custom-call | tf_op jit(solution)/shard_map/layer/pallas_call | solution.py:706
  152.5 1.7 %copy.19 = bf16[256,512]{1,0:T(8,128)(2,1)} copy(bf16[256,512]{1,0:T(8,128)(2,1)} %layer.1) | data formatting | bytes 524288
where the time goes:
time: 154 us
  Pallas kernels  153 us (99%)
  local copies, waits for them, and re-layouts  1.67 us (1%)
    pallas_call x1, Pallas kernels, head_per_device(): pl.pallas_call(functools.partial(layer_kernel, count, capacity), out_shap...  109 us
    pallas_call x1, Pallas kernels, head_per_device(): pl.pallas_call(functools.partial(spread_kernel, count, width), out_shape=...  26.1 us
    pallas_call x1, Pallas kernels, head_per_device(): pl.pallas_call(functools.partial(attend_kernel, (width // 2) ** (-0.5)),...  17.1 us

commit v1 on v0

--- a/solution.py
+++ b/solution.py
@@ -194,18 +194,47 @@
     pl.semaphore_wait(barrier, len(devices))
 
 
+def fold_axes(me, col):
+    core = lax.rem(me, 2)
+    return flip(col, 2 - core, 4), flip(col, 1 + core, 4), flip(col, jnp.int32(3), 4)
+
+
 def spread_kernel(
-    count, width, q_ref, k_ref, v_ref, doc_ref, out_ref, docs_ref, pack, send, recv, dsend, drecv
+    count,
+    width,
+    q_ref,
+    k_ref,
+    v_ref,
+    doc_ref,
+    down_hbm,
+    sdown_hbm,
+    out_ref,
+    docs_ref,
+    down_out,
+    sdown_out,
+    pack,
+    send,
+    recv,
+    dsend,
+    drecv,
+    wsend,
+    wrecv,
 ):
     me, col = lax.axis_index("sp"), lax.axis_index("tp")
     rows = q_ref.shape[0]
     half = rows // 2
     peers = [(flip(me, jnp.int32(k), count), col) for k in range(count)]
+    _, fold, across = fold_axes(me, col)
+    swaps = [
+        remote(src.at[quarter], dst.at[i], wsend.at[j, i], wrecv.at[j, i], (me, fold))
+        for j, (src, dst) in enumerate(((down_hbm, down_out), (sdown_hbm, sdown_out)))
+        for i, quarter in enumerate((fold, across))
+    ]
     for h in range(count):
         cut = slice(h * width, (h + 1) * width)
         pack[h, :rows, :] = jnp.concatenate([q_ref[:, cut], k_ref[:, cut]], axis=1)
         pack[h, rows:, :] = jnp.concatenate([v_ref[:half, cut], v_ref[half:, cut]], axis=1)
-    greet(peers[1:])
+    greet(peers[1:] + [(me, fold)])
     copies = []
     for k in reversed(range(1, count)):
         there = peers[k]
@@ -213,9 +242,11 @@
         copies.append(remote(pack.at[there[0]], out_ref.at[me], send.at[k], recv.at[k], there))
         copies[-2].start()
         copies[-1].start()
+    for swap in swaps:
+        swap.start()
     out_ref[me] = pack[me]
     docs_ref[me] = doc_ref[...]
-    for copy in copies:
+    for copy in copies + swaps:
         copy.wait()
 
 
@@ -333,27 +364,32 @@
     proj_hbm,
     sgate_hbm,
     sup_hbm,
-    sdown_hbm,
     gate_hbm,
     up_hbm,
+    sdown_hbm,
     down_hbm,
+    sdown_far_hbm,
+    down_far_hbm,
     out_ref,
     proj,
     sgate,
     sup,
-    sdown,
     gate,
     up,
+    sdown,
     down,
     held,
     head_buf,
     hidden_buf,
     normed,
     shared_buf,
+    shared_part,
     onehot,
     outgoing,
     rows_in,
     acts,
+    parts,
+    kept,
     made,
     back,
     shared_cols,
@@ -362,6 +398,8 @@
     hrecv,
     gsend,
     grecv,
+    fsend,
+    frecv,
     zsend,
     zrecv,
     rsend,
@@ -372,6 +410,7 @@
     half = rows // 2
     width = heads_ref.shape[2] // 2
     f32 = jnp.float32
+    meet, fold, _ = fold_axes(me, col)
     loads = [
         pltpu.make_async_copy(a, b, load_sem.at[i])
         for i, (a, b) in enumerate(
@@ -381,8 +420,12 @@
                 (sup_hbm, sup),
                 (gate_hbm, gate),
                 (up_hbm, up),
-                (sdown_hbm, sdown),
-                (down_hbm, down),
+                (sdown_hbm.at[col], sdown.at[0, 0]),
+                (sdown_hbm.at[meet], sdown.at[0, 1]),
+                (sdown_far_hbm, sdown.at[1]),
+                (down_hbm.at[col], down.at[0, 0]),
+                (down_hbm.at[meet], down.at[0, 1]),
+                (down_far_hbm, down.at[1]),
             )
         )
     ]
@@ -431,7 +474,15 @@
         for copy in direct(buf, row, index) + relays(buf, row, index):
             copy.wait_send()
 
-    row_head, row_hidden, row_shared = 2 * count, 2 * count + 2, 2 * count + 4
+    def join(buf, row, index=()):
+        own, other = buf.at[(0,) + index], buf.at[(1,) + index]
+        return remote(own, other, fsend.at[row, 0], frecv.at[row, 0], (me, meet))
+
+    def hand_over(buf, row, index=()):
+        own, other = buf.at[(0,) + index], buf.at[(1,) + index]
+        return remote(own, other, fsend.at[row, 1], frecv.at[row, 1], (me, fold))
+
+    row_head, row_hidden, row_shared = count, count + 2, count
 
     head_copies = []
     for k in reversed(range(1, count)):
@@ -487,20 +538,6 @@
         span = slice(h * half, (h + 1) * half)
         hidden_buf[0, h] = (stream_ref[span, :].astype(f32) + total).astype(jnp.bfloat16)
         offer(hidden_buf, row_hidden + h, (h,))
-    for h in range(2):
-        pass_on(hidden_buf, row_hidden + h, (h,))
-    for h in range(2):
-        finish(hidden_buf, row_hidden + h, (h,))
-        squares = jnp.zeros((half, cols), f32)
-        for j in range(4):
-            wide = hidden_buf[j, h].astype(f32)
-            squares = squares + wide * wide
-        mean = jnp.sum(squares, axis=1, keepdims=True) / (4 * cols)
-        scale = lax.rsqrt(mean + epsilon)
-        span = slice(h * half, (h + 1) * half)
-        for j in range(4):
-            wide = hidden_buf[j, h].astype(f32)
-            normed[j, span, :] = (wide * scale * gain_ref[side[j]]).astype(jnp.bfloat16)
 
     def dispatch_far(k):
         return remote(outgoing.at[0, k], rows_in.at[0, k], zsend.at[k], zrecv.at[k], peer(k))
@@ -509,18 +546,52 @@
         return remote(outgoing.at[:, k], rows_in.at[:, k], zsend.at[k], zrecv.at[k], peer(k))
 
     def chosen(k, j):
-        return jnp.dot(onehot[k], normed[j], preferred_element_type=f32).astype(jnp.bfloat16)
+        block = hidden_buf[j].reshape(rows, cols)
+        return jnp.dot(onehot[k], block, preferred_element_type=f32).astype(jnp.bfloat16)
 
     for k in range(4, count):
         outgoing[0, k] = chosen(k, 0)
         dispatch_far(jnp.int32(k)).start()
+    for h in range(2):
+        pass_on(hidden_buf, row_hidden + h, (h,))
+
+    def scaled(blocks):
+        wide = [block.astype(f32) for block in blocks]
+        squares = wide[0] * wide[0]
+        for block in wide[1:]:
+            squares = squares + block * block
+        scale = lax.rsqrt(jnp.sum(squares, axis=1, keepdims=True) / (4 * cols) + epsilon)
+        return [
+            (block * scale * gain_ref[side[j]]).astype(jnp.bfloat16)
+            for j, block in enumerate(wide)
+        ]
+
+    def gated_pair(blocks, first, second):
+        gated, lifted = [
+            sum(jnp.dot(block, w[side[j]], preferred_element_type=f32) for j, block in enumerate(blocks))
+            for w in (first, second)
+        ]
+        return (jax.nn.silu(gated) * lifted).astype(jnp.bfloat16)
+
+    for h in range(2):
+        finish(hidden_buf, row_hidden + h, (h,))
     for j in range(4):
         outgoing[j, 1] = chosen(1, j)
     dispatch_near(jnp.int32(1)).start()
+    for k in (2, 3):
+        for j in range(4):
+            outgoing[j, k] = chosen(k, j)
+        dispatch_near(jnp.int32(k)).start()
     for j in range(4):
         rows_in[j, 0] = chosen(0, j)
+    for h in range(2):
+        span = slice(h * half, (h + 1) * half)
+        for j, block in enumerate(scaled([hidden_buf[j, h] for j in range(4)])):
+            normed[j, span, :] = block
     for load in loads[1:]:
         load.wait()
+    dispatch_far(jnp.int32(4)).wait_recv()
+    offer(rows_in, 4, (4,))
 
     def give_back(k):
         return remote(made.at[k], back.at[k], rsend.at[k], rrecv.at[k], peer(k))
@@ -542,69 +613,60 @@
         @pl.when(i < count)
         def _():
             k = turn(i)
-            gated = jnp.zeros((capacity, cols), f32)
-            lifted = jnp.zeros((capacity, cols), f32)
-            for j in range(4):
-                gated = gated + jnp.dot(rows_in[j, k], gate[side[j]], preferred_element_type=f32)
-                lifted = lifted + jnp.dot(rows_in[j, k], up[side[j]], preferred_element_type=f32)
-            acts[0, k] = (jax.nn.silu(gated) * lifted).astype(jnp.bfloat16)
-            offer(acts, count + k, (k,))
+            acts[0, k] = gated_pair(scaled([rows_in[j, k] for j in range(4)]), gate, up)
+            join(acts, k, (k,)).start()
 
         @pl.when(i == 0)
         def _():
-            for k in (2, 3):
-                for j in range(4):
-                    outgoing[j, k] = chosen(k, j)
-                dispatch_near(jnp.int32(k)).start()
-            gated = jnp.zeros((rows, cols), f32)
-            lifted = jnp.zeros((rows, cols), f32)
-            for j in range(4):
-                gated = gated + jnp.dot(normed[j], sgate[side[j]], preferred_element_type=f32)
-                lifted = lifted + jnp.dot(normed[j], sup[side[j]], preferred_element_type=f32)
-            shared_buf[0] = (jax.nn.silu(gated) * lifted).astype(jnp.bfloat16)
-            offer(shared_buf, row_shared)
+            shared_buf[0] = gated_pair([normed[j] for j in range(4)], sgate, sup)
+            join(shared_buf, row_shared).start()
+
+        @pl.when(i < count - 5)
+        def _():
+            dispatch_far(i + 5).wait_recv()
+            offer(rows_in, i + 5, (i + 5,))
 
         @pl.when(i < count - 4)
         def _():
-            dispatch_far(i + 4).wait_recv()
-            offer(rows_in, i + 4, (i + 4,))
+            pass_on(rows_in, i + 4, (i + 4,))
 
         @pl.when((i >= 1) & (i < count + 1))
         def _():
             k = turn(i - 1)
-            pass_on(acts, count + k, (k,))
-
-        @pl.when((i >= 1) & (i < count - 3))
-        def _():
-            pass_on(rows_in, i + 3, (i + 3,))
+            join(acts, k, (k,)).wait_recv()
+            own, other = [
+                jnp.dot(acts[0, k], down[c, 0], preferred_element_type=f32)
+                + jnp.dot(acts[1, k], down[c, 1], preferred_element_type=f32)
+                for c in range(2)
+            ]
+            parts[0, k] = other.astype(jnp.bfloat16)
+            hand_over(parts, k, (k,)).start()
+            kept[k] = own
 
         @pl.when(i == 1)
         def _():
-            pass_on(shared_buf, row_shared)
-
-        @pl.when(i == 4)
-        def _():
-            finish(shared_buf, row_shared)
-            cols_sum = jnp.zeros((rows, cols), f32)
-            for j in range(4):
-                cols_sum = cols_sum + jnp.dot(
-                    shared_buf[j], sdown[side[j]], preferred_element_type=f32
-                )
-            shared_cols[...] = cols_sum
+            join(shared_buf, row_shared).wait_recv()
+            own, other = [
+                jnp.dot(shared_buf[0], sdown[c, 0], preferred_element_type=f32)
+                + jnp.dot(shared_buf[1], sdown[c, 1], preferred_element_type=f32)
+                for c in range(2)
+            ]
+            shared_part[0] = other.astype(jnp.bfloat16)
+            hand_over(shared_part, row_shared).start()
+            shared_cols[...] = own
 
         @pl.when(i >= 2)
         def _():
             k = turn(i - 2)
-            finish(acts, count + k, (k,))
-            result = jnp.zeros((capacity, cols), f32)
-            for j in range(4):
-                result = result + jnp.dot(acts[j, k], down[side[j]], preferred_element_type=f32)
-            made[k] = result.astype(jnp.bfloat16)
+            hand_over(parts, k, (k,)).wait_recv()
+            made[k] = (kept[k] + parts[1, k].astype(f32)).astype(jnp.bfloat16)
 
             @pl.when(k > 0)
             def _():
                 give_back(k).start()
 
+    hand_over(shared_part, row_shared).wait_recv()
+    shared_cols[...] = shared_cols[...] + shared_part[1].astype(f32)
     back[0] = made[0]
     for p in range(count):
         k = p if p < 2 else (p + 2 if p < count - 2 else p - count + 4)
@@ -625,7 +687,8 @@
     for h in range(2):
         drain(head_buf, row_head + h, (h,))
         drain(hidden_buf, row_hidden + h, (h,))
-    drain(shared_buf, row_shared)
+    join(shared_buf, row_shared).wait_send()
+    hand_over(shared_part, row_shared).wait_send()
 
     @pl.loop(4, count)
     def _(k):
@@ -638,7 +701,8 @@
 
     @pl.loop(0, count)
     def _(k):
-        drain(acts, count + k, (k,))
+        join(acts, k, (k,)).wait_send()
+        hand_over(parts, k, (k,)).wait_send()
 
         @pl.when(k > 0)
         def _():
@@ -670,24 +734,30 @@
     capacity = 2 * rows * routes.shape[1] // count
     bf16, f32 = jnp.bfloat16, jnp.float32
     dma = pltpu.SemaphoreType.DMA
-    qkv, docs = pl.pallas_call(
+    split = lambda weight: weight.reshape(sides, weight.shape[-2] // sides, weight.shape[-1])
+    down, sdown = split(expert_down[0]), split(shared_down)
+    qkv, docs, down_far, sdown_far = pl.pallas_call(
         functools.partial(spread_kernel, count, width),
         out_shape=(
             jax.ShapeDtypeStruct((count, rows + rows // 2, 2 * width), bf16),
             jax.ShapeDtypeStruct((count, 1, rows), jnp.int32),
+            jax.ShapeDtypeStruct((2, cols, cols), bf16),
+            jax.ShapeDtypeStruct((2, cols, cols), bf16),
         ),
-        in_specs=[VMEM] * 4,
-        out_specs=(VMEM, VMEM),
+        in_specs=[VMEM] * 4 + [ANY] * 2,
+        out_specs=(VMEM, VMEM, ANY, ANY),
         scratch_shapes=[
             pltpu.VMEM((count, rows + rows // 2, 2 * width), bf16),
             dma((count,)),
             dma((count,)),
             dma((count,)),
             dma((count,)),
+            dma((2, 2)),
+            dma((2, 2)),
         ],
         compiler_params=pltpu.CompilerParams(collective_id=0, has_side_effects=True),
         name="spread_heads",
-    )(query_pairs, key_pairs, value_rows, doc_ids.reshape(1, rows))
+    )(query_pairs, key_pairs, value_rows, doc_ids.reshape(1, rows), down, sdown)
     heads = pl.pallas_call(
         functools.partial(attend_kernel, (width // 2) ** (-0.5)),
         out_shape=jax.ShapeDtypeStruct((count, rows // 2, 2 * width), bf16),
@@ -701,32 +771,38 @@
         docs,
         head_gain.reshape(1, width),
     )
-    split = lambda weight: weight.reshape(sides, weight.shape[-2] // sides, weight.shape[-1])
     weight_shape = (sides, cols, cols)
+    slots = (count, capacity, cols)
     return pl.pallas_call(
         functools.partial(layer_kernel, count, capacity),
         out_shape=jax.ShapeDtypeStruct((rows, cols), bf16),
-        in_specs=[VMEM] * 5 + [ANY] * 7,
+        in_specs=[VMEM] * 5 + [ANY] * 9,
         out_specs=VMEM,
-        scratch_shapes=[pltpu.VMEM(weight_shape, bf16)] * 7
+        scratch_shapes=[pltpu.VMEM(weight_shape, bf16)] * 5
+        + [pltpu.VMEM((2, 2, cols, cols), bf16)] * 2
         + [
             pltpu.VMEM((count, rows // 2, 2 * width), bf16),
             pltpu.VMEM((sides, 2, rows // 2, cols), bf16),
             pltpu.VMEM((sides, 2, rows // 2, cols), bf16),
             pltpu.VMEM((sides, rows, cols), bf16),
-            pltpu.VMEM((sides, rows, cols), bf16),
+            pltpu.VMEM((2, rows, cols), bf16),
+            pltpu.VMEM((2, rows, cols), bf16),
             pltpu.VMEM((count, capacity, rows), bf16),
-            pltpu.VMEM((sides, count, capacity, cols), bf16),
-            pltpu.VMEM((sides, count, capacity, cols), bf16),
-            pltpu.VMEM((sides, count, capacity, cols), bf16),
-            pltpu.VMEM((count, capacity, cols), bf16),
-            pltpu.VMEM((count, capacity, cols), bf16),
+            pltpu.VMEM((sides,) + slots, bf16),
+            pltpu.VMEM((sides,) + slots, bf16),
+            pltpu.VMEM((2,) + slots, bf16),
+            pltpu.VMEM((2,) + slots, bf16),
+            pltpu.VMEM(slots, f32),
+            pltpu.VMEM(slots, bf16),
+            pltpu.VMEM(slots, bf16),
             pltpu.VMEM((rows, cols), f32),
-            dma((7,)),
-            dma((count,)),
-            dma((count,)),
-            dma((2 * count + 5, 4)),
-            dma((2 * count + 5, 4)),
+            dma((11,)),
+            dma((count,)),
+            dma((count,)),
+            dma((count + 4, 4)),
+            dma((count + 4, 4)),
+            dma((count + 1, 2)),
+            dma((count + 1, 2)),
             dma((count,)),
             dma((count,)),
             dma((count,)),
@@ -745,10 +821,12 @@
         split(out_proj),
         split(shared_gate),
         split(shared_up),
-        split(shared_down),
         split(expert_gate[0]),
         split(expert_up[0]),
-        split(expert_down[0]),
+        sdown,
+        down,
+        sdown_far,
+        down_far,
     )
 
 

time: 154 us -> 147 us (0.955)
  Pallas kernels: 153 us -> 146 us
    pallas_call x1, Pallas kernels: 109 us -> 94.8 us  [head_per_device(): pl.pallas_call(functools.partial(layer_kernel, count, capacity), out_shap...]
    pallas_call x1, Pallas kernels: 26.1 us -> 33.6 us  [head_per_device(): pl.pallas_call(functools.partial(spread_kernel, count, width), out_shape=...]
where the time goes in v1:
time: 147 us
  Pallas kernels  146 us (99%)
  local copies, waits for them, and re-layouts  1.67 us (1%)
    pallas_call x1, Pallas kernels, head_per_device(): pl.pallas_call(functools.partial(layer_kernel, count, capacity), out_shap...  94.8 us
    pallas_call x1, Pallas kernels, head_per_device(): pl.pallas_call(functools.partial(spread_kernel, count, width), out_shape=...  33.6 us
    pallas_call x1, Pallas kernels, head_per_device(): pl.pallas_call(functools.partial(attend_kernel, (width // 2) ** (-0.5)),...  17.1 us

profile of v1, /device:TPU:0, one launch (start us, length us, event | category | flops | bytes accessed | tf_op | source)
XLA Modules:
  0.0 147.2 jit_solution(3788732120770548457)
XLA Ops:
  0.0 33.6 %spread_heads.1 = (bf16[8,384,128]{2,1,0:T(8,128)(2,1)}, s32[8,1,256]{2,1,0:T(1,128)}, bf16[2,512,512]{2,1,0:T(8,128)(2,1)}, bf16[2,512,512]{2,1,0:T(8,128)(2,1)}) custom-call(bf16[256,512]{1,0:T(8,128)(2,1)} %q_ref.1, bf16[256,512]{1,0:T(8,128)(2,1)} %k_ref.1, bf16[256,512]{1,0:T(8,128)(2,1)} %v_ref.1, s32[1,256]{1,0:T(1,128)} %bitcast.24, ...), custom_call_target="tpu_custom_call" | custom-call | tf_op jit(solution)/shard_map/spread_heads/pallas_call | solution.py:739
  33.6 17.1 %attend.1.heads_ref = bf16[8,128,128]{2,1,0:T(8,128)(2,1)} custom-call(f32[8]{0:T(128)} %lam_ref.1, bf16[8,384,128]{2,1,0:T(8,128)(2,1)} %get-tuple-element.9.qkv_ref, s32[8,1,256]{2,1,0:T(1,128)} %get-tuple-element.10.doc_ref, f32[1,64]{1,0:T(1,128)} %bitcast.25), custom_call_target="tpu_custom_call" | custom-call | tf_op jit(solution)/shard_map/attend/pallas_call | solution.py:761
  50.7 94.8 %layer.1 = bf16[256,512]{1,0:T(8,128)(2,1)} custom-call(bf16[8,128,128]{2,1,0:T(8,128)(2,1)} %attend.1.heads_ref, bf16[256,512]{1,0:T(8,128)(2,1)} %stream_ref.1, f32[4,1,512]{2,1,0:T(1,128)} %bitcast.21, s32[2,256]{1,0:T(2,128)} %bitcast.22, f32[2,256]{1,0:T(2,128)} %bitcast.23, bf16[4,512,512]{2,1,0:T(8,128)(2,1)} %bitcast.16, ...), custom_call_target="tpu_custom_call" | custom-call | tf_op jit(solution)/shard_map/layer/pallas_call | solution.py:776
  145.6 1.7 %copy.19 = bf16[256,512]{1,0:T(8,128)(2,1)} copy(bf16[256,512]{1,0:T(8,128)(2,1)} %layer.1) | data formatting | bytes 524288

commit v2 on v1

--- a/solution.py
+++ b/solution.py
@@ -199,164 +199,16 @@
     return flip(col, 2 - core, 4), flip(col, 1 + core, 4), flip(col, jnp.int32(3), 4)
 
 
-def spread_kernel(
+def layer_kernel(
     count,
-    width,
+    capacity,
+    scaling,
+    lam_ref,
     q_ref,
     k_ref,
     v_ref,
     doc_ref,
-    down_hbm,
-    sdown_hbm,
-    out_ref,
-    docs_ref,
-    down_out,
-    sdown_out,
-    pack,
-    send,
-    recv,
-    dsend,
-    drecv,
-    wsend,
-    wrecv,
-):
-    me, col = lax.axis_index("sp"), lax.axis_index("tp")
-    rows = q_ref.shape[0]
-    half = rows // 2
-    peers = [(flip(me, jnp.int32(k), count), col) for k in range(count)]
-    _, fold, across = fold_axes(me, col)
-    swaps = [
-        remote(src.at[quarter], dst.at[i], wsend.at[j, i], wrecv.at[j, i], (me, fold))
-        for j, (src, dst) in enumerate(((down_hbm, down_out), (sdown_hbm, sdown_out)))
-        for i, quarter in enumerate((fold, across))
-    ]
-    for h in range(count):
-        cut = slice(h * width, (h + 1) * width)
-        pack[h, :rows, :] = jnp.concatenate([q_ref[:, cut], k_ref[:, cut]], axis=1)
-        pack[h, rows:, :] = jnp.concatenate([v_ref[:half, cut], v_ref[half:, cut]], axis=1)
-    greet(peers[1:] + [(me, fold)])
-    copies = []
-    for k in reversed(range(1, count)):
-        there = peers[k]
-        copies.append(remote(doc_ref, docs_ref.at[me], dsend.at[k], drecv.at[k], there))
-        copies.append(remote(pack.at[there[0]], out_ref.at[me], send.at[k], recv.at[k], there))
-        copies[-2].start()
-        copies[-1].start()
-    for swap in swaps:
-        swap.start()
-    out_ref[me] = pack[me]
-    docs_ref[me] = doc_ref[...]
-    for copy in copies + swaps:
-        copy.wait()
-
-
-def attend_kernel(
-    scaling, lam_ref, qkv_ref, doc_ref, gain_ref, out_ref, turned
-):
-    count, rows = doc_ref.shape[0], doc_ref.shape[2]
-    half = rows // 2
-    width = gain_ref.shape[1]
-    weight = lam_ref[lax.axis_index("sp")]
-    gains = jnp.concatenate([gain_ref[...], gain_ref[...]], axis=1)
-    doc_rows = jnp.concatenate([doc_ref[b] for b in range(count)], axis=0).astype(jnp.float32)
-    doc_cols = jnp.transpose(doc_rows)
-    key_width = width // 2
-    lanes = lax.broadcasted_iota(jnp.int32, (rows, 2 * width), 1)
-    factor = scaling * math.log2(math.e)
-
-    @pl.loop(0, count)
-    def _(b):
-        turned[b] = jnp.transpose(qkv_ref[b, rows:, :].astype(jnp.float32)).astype(jnp.bfloat16)
-
-    @pl.loop(0, count)
-    def _(b):
-        moved = pltpu.roll(qkv_ref[b, :rows, :].astype(jnp.float32), width, 1)
-        queries = [
-            jnp.where(
-                (lanes >= width + m * key_width) & (lanes < width + (m + 1) * key_width),
-                moved,
-                0.0,
-            ).astype(jnp.bfloat16)
-            for m in range(2)
-        ]
-        own_docs = doc_ref[b].astype(jnp.float32)
-        earlier = jnp.zeros((rows, rows), jnp.float32)
-        for kb in range(count):
-            earlier = earlier + jnp.where(doc_cols[:, kb : kb + 1] < own_docs, 1.0, 0.0)
-        earlier = jnp.sum(earlier, axis=0, keepdims=True)
-        starts = earlier.astype(jnp.int32)
-        first = lax.div(jnp.min(earlier).astype(jnp.int32), rows)
-        query_pos = b * rows + lax.broadcasted_iota(jnp.int32, (1, rows), 1)
-
-        def step(i, carried):
-            tiles = []
-            for part in range(2):
-                kb = b - 2 * i - part
-                key_pos = kb * rows + lax.broadcasted_iota(jnp.int32, (rows, rows), 0)
-                allowed = (key_pos <= query_pos) & (key_pos >= starts)
-                tiles.append((jnp.maximum(kb, 0), allowed))
-            scores = [
-                [
-                    jnp.where(
-                        allowed,
-                        lax.dot_general(
-                            qkv_ref[kb, :rows, :], queries[m], (((1,), (1,)), ((), ())),
-                            preferred_element_type=jnp.float32,
-                        )
-                        * factor,
-                        floor_score,
-                    )
-                    for kb, allowed in tiles
-                ]
-                for m in range(2)
-            ]
-            out = []
-            for m in range(2):
-                best, denom, numer = carried[m]
-                tallest = jnp.max(jnp.maximum(*scores[m]), axis=0, keepdims=True)
-                new_best = jnp.maximum(best, tallest)
-                fade = jnp.exp2(best - new_best)
-                weights = [jnp.exp2(tile - new_best) for tile in scores[m]]
-                denom = denom * fade + jnp.sum(weights[0] + weights[1], axis=0, keepdims=True)
-                numer = numer * fade
-                for (kb, _), tile in zip(tiles, weights):
-                    rounded = tile.astype(jnp.bfloat16)
-                    numer = (
-                        numer
-                        + jnp.dot(
-                            turned[kb, :width, :], rounded[:half],
-                            preferred_element_type=jnp.float32,
-                        )
-                        + jnp.dot(
-                            turned[kb, width:, :], rounded[half:],
-                            preferred_element_type=jnp.float32,
-                        )
-                    )
-                out.append((new_best, denom, numer))
-            return tuple(out)
-
-        begin = tuple(
-            (
-                jnp.full((1, rows), floor_score, jnp.float32),
-                jnp.zeros((1, rows), jnp.float32),
-                jnp.zeros((width, rows), jnp.float32),
-            )
-            for _ in range(2)
-        )
-        done = lax.fori_loop(0, lax.div(b - first, 2) + 1, step, begin)
-        heard = [numer / denom for _, denom, numer in done]
-        contrast = heard[0] - weight * heard[1]
-        contrast = contrast * lax.rsqrt(
-            jnp.mean(contrast * contrast, axis=0, keepdims=True) + epsilon
-        )
-        stacked = jnp.concatenate([contrast[:, :half], contrast[:, half:]], axis=0)
-        out_ref[b] = (jnp.transpose(stacked) * gains).astype(jnp.bfloat16)
-
-
-def layer_kernel(
-    count,
-    capacity,
-    heads_ref,
+    head_gain_ref,
     stream_ref,
     gain_ref,
     routes_ref,
@@ -368,9 +220,18 @@
     up_hbm,
     sdown_hbm,
     down_hbm,
-    sdown_far_hbm,
-    down_far_hbm,
     out_ref,
+    pack,
+    qkv,
+    docs,
+    doc_cols,
+    queries,
+    turned,
+    best_ref,
+    denom_ref,
+    numer_ref,
+    head_out,
+    portions,
     proj,
     sgate,
     sup,
@@ -394,6 +255,10 @@
     back,
     shared_cols,
     load_sem,
+    xsend,
+    xrecv,
+    wsend,
+    wrecv,
     hsend,
     hrecv,
     gsend,
@@ -408,9 +273,10 @@
     me, col = lax.axis_index("sp"), lax.axis_index("tp")
     rows, cols = stream_ref.shape
     half = rows // 2
-    width = heads_ref.shape[2] // 2
+    width = head_gain_ref.shape[1]
+    key_width = width // 2
     f32 = jnp.float32
-    meet, fold, _ = fold_axes(me, col)
+    meet, fold, across = fold_axes(me, col)
     loads = [
         pltpu.make_async_copy(a, b, load_sem.at[i])
         for i, (a, b) in enumerate(
@@ -422,10 +288,8 @@
                 (up_hbm, up),
                 (sdown_hbm.at[col], sdown.at[0, 0]),
                 (sdown_hbm.at[meet], sdown.at[0, 1]),
-                (sdown_far_hbm, sdown.at[1]),
                 (down_hbm.at[col], down.at[0, 0]),
                 (down_hbm.at[meet], down.at[0, 1]),
-                (down_far_hbm, down.at[1]),
             )
         )
     ]
@@ -434,6 +298,10 @@
     side = [flip(col, jnp.int32(j), 4) for j in range(4)]
     peer = lambda k: (flip(me, k, count), col)
     near_x, near_y = (me, side[1]), (me, side[2])
+    for h in range(count):
+        cut = slice(h * width, (h + 1) * width)
+        pack[h, :rows, :] = jnp.concatenate([q_ref[:, cut], k_ref[:, cut]], axis=1)
+        pack[h, rows:, :] = jnp.concatenate([v_ref[:half, cut], v_ref[half:, cut]], axis=1)
     greet([peer(jnp.int32(k)) for k in range(1, count)] + [near_x, near_y])
 
     def direct(buf, row, index):
@@ -484,14 +352,32 @@
 
     row_head, row_hidden, row_shared = count, count + 2, count
 
-    head_copies = []
-    for k in reversed(range(1, count)):
-        there = peer(jnp.int32(k))
-        head_copies.append(
-            remote(heads_ref.at[there[0]], held.at[me], hsend.at[k], hrecv.at[k], there)
-        )
-        head_copies[-1].start()
-    held[me] = heads_ref[me]
+    def exchange(k):
+        there = peer(k)
+        return (
+            remote(doc_ref, docs.at[me], xsend.at[0, k], xrecv.at[0, k], there),
+            remote(pack.at[there[0]], qkv.at[me], xsend.at[1, k], xrecv.at[1, k], there),
+        )
+
+    def head_copy(k):
+        there = peer(k)
+        return remote(head_out.at[there[0]], held.at[me], hsend.at[k], hrecv.at[k], there)
+
+    swaps = [
+        remote(src.at[quarter], dst.at[1, i], wsend.at[j, i], wrecv.at[j, i], (me, fold))
+        for j, (src, dst) in enumerate(((down_hbm, down), (sdown_hbm, sdown)))
+        for i, quarter in enumerate((fold, across))
+    ]
+    for k in range(1, count):
+        for copy in exchange(jnp.int32(k)):
+            copy.start()
+    for swap in swaps:
+        swap.start()
+    qkv[me] = pack[me]
+    docs[me] = doc_ref[...]
+    best_ref[...] = jnp.full(best_ref.shape, floor_score, f32)
+    denom_ref[...] = jnp.zeros(denom_ref.shape, f32)
+    numer_ref[...] = jnp.zeros(numer_ref.shape, f32)
 
     near = routes_ref[...] ^ me
     lane = lax.broadcasted_iota(jnp.int32, (128, rows), 0)
@@ -513,10 +399,111 @@
     portion = jnp.where(hits[0], weight_ref[0:1, :], 0.0) + jnp.where(
         hits[1], weight_ref[1:2, :], 0.0
     )
-    portions = jnp.transpose(portion)
-
-    for copy in head_copies:
-        copy.wait_recv()
+    portions[...] = jnp.transpose(portion)
+
+    weight = lam_ref[me]
+    gains = jnp.concatenate([head_gain_ref[...], head_gain_ref[...]], axis=1)
+    factor = scaling * math.log2(math.e)
+    lanes = lax.broadcasted_iota(jnp.int32, (rows, 2 * width), 1)
+
+    @pl.loop(0, count)
+    def _(i):
+        j = flip(me, i, count)
+
+        @pl.when(i > 0)
+        def _():
+            for copy in exchange(i):
+                copy.wait_recv()
+
+        values = jnp.transpose(qkv[j, rows:, :].astype(f32)).astype(jnp.bfloat16)
+        turned[j] = jnp.concatenate([values[:width], values[width:]], axis=1)
+        moved = pltpu.roll(qkv[j, :rows, :].astype(f32), width, 1)
+        for m in range(2):
+            begin = width + m * key_width
+            inside = (lanes >= begin) & (lanes < begin + key_width)
+            queries[j, m] = jnp.where(inside, moved, 0.0).astype(jnp.bfloat16)
+        doc_cols[j] = jnp.transpose(jnp.broadcast_to(docs[j].astype(f32), (8, rows)))
+
+        def pair_of_tiles(step, carried):
+            ahead = lax.broadcasted_iota(jnp.int32, (rows, rows), 0) - lax.broadcasted_iota(
+                jnp.int32, (rows, rows), 1
+            )
+            tiles = []
+            for part in range(2):
+                second = 2 * step + part
+                other = flip(me, jnp.minimum(second, i), count)
+                q, k = jnp.maximum(j, other), jnp.minimum(j, other)
+                limit = jnp.where(second <= i, (q - k) * rows, -rows)
+                allowed = (ahead <= limit) & (doc_cols[k][:, 0:1] == docs[q].astype(f32))
+                tiles.append((q, k, allowed))
+            scores = [
+                [
+                    jnp.where(
+                        allowed,
+                        lax.dot_general(
+                            qkv[k, :rows, :], queries[q, m], (((1,), (1,)), ((), ())),
+                            preferred_element_type=f32,
+                        )
+                        * factor,
+                        floor_score,
+                    )
+                    for m in range(2)
+                ]
+                for q, k, allowed in tiles
+            ]
+            for part, (q, k, _) in enumerate(tiles):
+                for m in range(2):
+                    row = pl.ds(2 * part + m, 1)
+                    tile = scores[part][m]
+                    best = best_ref[q, row, :]
+                    new_best = jnp.maximum(best, jnp.max(tile, axis=0, keepdims=True))
+                    fade = jnp.exp2(best - new_best)
+                    weights = jnp.exp2(tile - new_best)
+                    best_ref[q, row, :] = new_best
+                    denom_ref[q, row, :] = denom_ref[q, row, :] * fade + jnp.sum(
+                        weights, axis=0, keepdims=True
+                    )
+                    numer_ref[q, 2 * part + m] = numer_ref[q, 2 * part + m] * fade + jnp.dot(
+                        turned[k], weights.astype(jnp.bfloat16), preferred_element_type=f32
+                    )
+            return carried
+
+        lax.fori_loop(0, lax.div(i, 2) + 1, pair_of_tiles, 0)
+
+    @pl.loop(0, count)
+    def _(i):
+        k = count - 1 - i
+        b = flip(me, k, count)
+        heard = []
+        for m in range(2):
+            bests = [best_ref[b, pl.ds(2 * part + m, 1), :] for part in range(2)]
+            top = jnp.maximum(*bests)
+            fades = [jnp.exp2(best - top) for best in bests]
+            denom, numer = [
+                first * fades[0] + second * fades[1]
+                for first, second in (
+                    [denom_ref[b, pl.ds(2 * part + m, 1), :] for part in range(2)],
+                    [numer_ref[b, 2 * part + m] for part in range(2)],
+                )
+            ]
+            heard.append(numer / denom)
+        contrast = heard[0] - weight * heard[1]
+        contrast = contrast * lax.rsqrt(
+            jnp.mean(contrast * contrast, axis=0, keepdims=True) + epsilon
+        )
+        stacked = jnp.concatenate([contrast[:, :half], contrast[:, half:]], axis=0)
+        head_out[b] = (jnp.transpose(stacked) * gains).astype(jnp.bfloat16)
+
+        @pl.when(k > 0)
+        def _():
+            head_copy(k).start()
+
+    held[me] = head_out[me]
+
+    @pl.loop(1, count)
+    def _(k):
+        head_copy(k).wait_recv()
+
     for pair in range(count // 2):
         first, second = held[2 * pair], held[2 * pair + 1]
         cut = slice(2 * pair * width, 2 * (pair + 1) * width)
@@ -590,6 +577,8 @@
             normed[j, span, :] = block
     for load in loads[1:]:
         load.wait()
+    for swap in swaps:
+        swap.wait_recv()
     dispatch_far(jnp.int32(4)).wait_recv()
     offer(rows_in, 4, (4,))
 
@@ -682,8 +671,8 @@
             jnp.bfloat16
         )
 
-    for copy in head_copies:
-        copy.wait_send()
+    for swap in swaps:
+        swap.wait_send()
     for h in range(2):
         drain(head_buf, row_head + h, (h,))
         drain(hidden_buf, row_hidden + h, (h,))
@@ -698,6 +687,12 @@
     @pl.loop(1, 4)
     def _(k):
         dispatch_near(k).wait_send()
+
+    @pl.loop(1, count)
+    def _(k):
+        head_copy(k).wait_send()
+        for copy in exchange(k):
+            copy.wait_send()
 
     @pl.loop(0, count)
     def _(k):
@@ -736,49 +731,27 @@
     dma = pltpu.SemaphoreType.DMA
     split = lambda weight: weight.reshape(sides, weight.shape[-2] // sides, weight.shape[-1])
     down, sdown = split(expert_down[0]), split(shared_down)
-    qkv, docs, down_far, sdown_far = pl.pallas_call(
-        functools.partial(spread_kernel, count, width),
-        out_shape=(
-            jax.ShapeDtypeStruct((count, rows + rows // 2, 2 * width), bf16),
-            jax.ShapeDtypeStruct((count, 1, rows), jnp.int32),
-            jax.ShapeDtypeStruct((2, cols, cols), bf16),
-            jax.ShapeDtypeStruct((2, cols, cols), bf16),
-        ),
-        in_specs=[VMEM] * 4 + [ANY] * 2,
-        out_specs=(VMEM, VMEM, ANY, ANY),
-        scratch_shapes=[
-            pltpu.VMEM((count, rows + rows // 2, 2 * width), bf16),
-            dma((count,)),
-            dma((count,)),
-            dma((count,)),
-            dma((count,)),
-            dma((2, 2)),
-            dma((2, 2)),
-        ],
-        compiler_params=pltpu.CompilerParams(collective_id=0, has_side_effects=True),
-        name="spread_heads",
-    )(query_pairs, key_pairs, value_rows, doc_ids.reshape(1, rows), down, sdown)
-    heads = pl.pallas_call(
-        functools.partial(attend_kernel, (width // 2) ** (-0.5)),
-        out_shape=jax.ShapeDtypeStruct((count, rows // 2, 2 * width), bf16),
-        in_specs=[SMEM, VMEM, VMEM, VMEM],
-        out_specs=VMEM,
-        scratch_shapes=[pltpu.VMEM((count, 2 * width, rows // 2), bf16)],
-        name="attend",
-    )(
-        contrast_lambda,
-        qkv,
-        docs,
-        head_gain.reshape(1, width),
-    )
     weight_shape = (sides, cols, cols)
     slots = (count, capacity, cols)
     return pl.pallas_call(
-        functools.partial(layer_kernel, count, capacity),
+        functools.partial(layer_kernel, count, capacity, (width // 2) ** (-0.5)),
         out_shape=jax.ShapeDtypeStruct((rows, cols), bf16),
-        in_specs=[VMEM] * 5 + [ANY] * 9,
+        in_specs=[SMEM] + [VMEM] * 9 + [ANY] * 7,
         out_specs=VMEM,
-        scratch_shapes=[pltpu.VMEM(weight_shape, bf16)] * 5
+        scratch_shapes=[
+            pltpu.VMEM((count, rows + rows // 2, 2 * width), bf16),
+            pltpu.VMEM((count, rows + rows // 2, 2 * width), bf16),
+            pltpu.VMEM((count, 1, rows), jnp.int32),
+            pltpu.VMEM((count, rows, 8), f32),
+            pltpu.VMEM((count, 2, rows, 2 * width), bf16),
+            pltpu.VMEM((count, width, rows), bf16),
+            pltpu.VMEM((count, 4, rows), f32),
+            pltpu.VMEM((count, 4, rows), f32),
+            pltpu.VMEM((count, 4, width, rows), f32),
+            pltpu.VMEM((count, rows // 2, 2 * width), bf16),
+            pltpu.VMEM((rows, 128), f32),
+        ]
+        + [pltpu.VMEM(weight_shape, bf16)] * 5
         + [pltpu.VMEM((2, 2, cols, cols), bf16)] * 2
         + [
             pltpu.VMEM((count, rows // 2, 2 * width), bf16),
@@ -796,7 +769,11 @@
             pltpu.VMEM(slots, bf16),
             pltpu.VMEM(slots, bf16),
             pltpu.VMEM((rows, cols), f32),
-            dma((11,)),
+            dma((9,)),
+            dma((2, count)),
+            dma((2, count)),
+            dma((2, 2)),
+            dma((2, 2)),
             dma((count,)),
             dma((count,)),
             dma((count + 4, 4)),
@@ -809,11 +786,16 @@
             dma((count,)),
         ],
         compiler_params=pltpu.CompilerParams(
-            collective_id=1, has_side_effects=True, vmem_limit_bytes=60 * 2**20
+            collective_id=0, has_side_effects=True, vmem_limit_bytes=60 * 2**20
         ),
         name="layer",
     )(
-        heads,
+        contrast_lambda,
+        query_pairs,
+        key_pairs,
+        value_rows,
+        doc_ids.reshape(1, rows),
+        head_gain.reshape(1, width),
         stream,
         norm_gain.reshape(sides, 1, cols),
         routes.T,
@@ -825,8 +807,6 @@
         split(expert_up[0]),
         sdown,
         down,
-        sdown_far,
-        down_far,
     )
 
 

time: 147 us -> 122 us (0.83)
  Pallas kernels: 146 us -> 120 us
    pallas_call x3 -> x1, Pallas kernels: 146 us -> 120 us  [head_per_device(): pl.pallas_call(functools.partial(layer_kernel, count, capacity, (width //...]
where the time goes in v2:
time: 122 us
  Pallas kernels  120 us (98%)
  local copies, waits for them, and re-layouts  1.67 us (1%)
    pallas_call x1, Pallas kernels, head_per_device(): pl.pallas_call(functools.partial(layer_kernel, count, capacity, (width //...  120 us

profile of v2, /device:TPU:0, one launch (start us, length us, event | category | flops | bytes accessed | tf_op | source)
XLA Modules:
  0.0 121.6 jit_solution(795985486334225615)
XLA Ops:
  0.0 119.9 %layer.1 = bf16[256,512]{1,0:T(8,128)(2,1)} custom-call(f32[8]{0:T(128)} %lam_ref.1, bf16[256,512]{1,0:T(8,128)(2,1)} %q_ref.1, bf16[256,512]{1,0:T(8,128)(2,1)} %k_ref.1, bf16[256,512]{1,0:T(8,128)(2,1)} %v_ref.1, s32[1,256]{1,0:T(1,128)} %bitcast.22, f32[1,64]{1,0:T(1,128)} %bitcast.23, bf16[256,512]{1,0:T(8,128)(2,1)} %stream_ref.1, ...), custom_call_target="tpu_custom_call" | custom-call | tf_op jit(solution)/shard_map/layer/pallas_call | solution.py:736
  119.9 1.7 %copy.19 = bf16[256,512]{1,0:T(8,128)(2,1)} copy(bf16[256,512]{1,0:T(8,128)(2,1)} %layer.1) | data formatting | bytes 524288

commit v3 on v2

--- a/solution.py
+++ b/solution.py
@@ -185,13 +185,6 @@
         device_id=device,
         device_id_type=MESH_ID,
     )
-
-
-def greet(devices):
-    barrier = pltpu.get_barrier_semaphore()
-    for device in devices:
-        pl.semaphore_signal(barrier, inc=1, device_id=device, device_id_type=MESH_ID)
-    pl.semaphore_wait(barrier, len(devices))
 
 
 def fold_axes(me, col):
@@ -253,6 +246,7 @@
     kept,
     made,
     back,
+    made_two,
     shared_cols,
     load_sem,
     xsend,
@@ -298,11 +292,15 @@
     side = [flip(col, jnp.int32(j), 4) for j in range(4)]
     peer = lambda k: (flip(me, k, count), col)
     near_x, near_y = (me, side[1]), (me, side[2])
+    friends = [peer(jnp.int32(k)) for k in range(1, count)] + [near_x, near_y]
+    barrier = pltpu.get_barrier_semaphore()
+    for device in friends:
+        pl.semaphore_signal(barrier, inc=1, device_id=device, device_id_type=MESH_ID)
     for h in range(count):
         cut = slice(h * width, (h + 1) * width)
         pack[h, :rows, :] = jnp.concatenate([q_ref[:, cut], k_ref[:, cut]], axis=1)
         pack[h, rows:, :] = jnp.concatenate([v_ref[:half, cut], v_ref[half:, cut]], axis=1)
-    greet([peer(jnp.int32(k)) for k in range(1, count)] + [near_x, near_y])
+    pl.semaphore_wait(barrier, len(friends))
 
     def direct(buf, row, index):
         own = buf.at[(0,) + index]
@@ -350,7 +348,7 @@
         own, other = buf.at[(0,) + index], buf.at[(1,) + index]
         return remote(own, other, fsend.at[row, 1], frecv.at[row, 1], (me, fold))
 
-    row_head, row_hidden, row_shared = count, count + 2, count
+    row_head, row_hidden, row_shared = count, count + count // 2, count
 
     def exchange(k):
         there = peer(k)
@@ -406,6 +404,35 @@
     factor = scaling * math.log2(math.e)
     lanes = lax.broadcasted_iota(jnp.int32, (rows, 2 * width), 1)
 
+    def conclude(k):
+        b = flip(me, k, count)
+        heard = []
+        for m in range(2):
+            bests = [best_ref[b, pl.ds(2 * part + m, 1), :] for part in range(2)]
+            top = jnp.maximum(*bests)
+            fades = [jnp.exp2(best - top) for best in bests]
+            denom, numer = [
+                first * fades[0] + second * fades[1]
+                for first, second in (
+                    [denom_ref[b, pl.ds(2 * part + m, 1), :] for part in range(2)],
+                    [numer_ref[b, 2 * part + m] for part in range(2)],
+                )
+            ]
+            heard.append(numer / denom)
+        contrast = heard[0] - weight * heard[1]
+        contrast = contrast * lax.rsqrt(
+            jnp.mean(contrast * contrast, axis=0, keepdims=True) + epsilon
+        )
+        stacked = jnp.concatenate([contrast[:, :half], contrast[:, half:]], axis=0)
+        head_out[b] = (jnp.transpose(stacked) * gains).astype(jnp.bfloat16)
+
+        @pl.when(k > 0)
+        def _():
+            head_copy(k).start()
+
+    layer_of = lax.div(me, 2)
+    lower = me < count // 2
+
     @pl.loop(0, count)
     def _(i):
         j = flip(me, i, count)
@@ -425,6 +452,7 @@
         doc_cols[j] = jnp.transpose(jnp.broadcast_to(docs[j].astype(f32), (8, rows)))
 
         def pair_of_tiles(step, carried):
+            step = lax.div(i, 2) - step
             ahead = lax.broadcasted_iota(jnp.int32, (rows, rows), 0) - lax.broadcasted_iota(
                 jnp.int32, (rows, rows), 1
             )
@@ -468,62 +496,63 @@
                     )
             return carried
 
-        lax.fori_loop(0, lax.div(i, 2) + 1, pair_of_tiles, 0)
-
-    @pl.loop(0, count)
-    def _(i):
-        k = count - 1 - i
-        b = flip(me, k, count)
-        heard = []
-        for m in range(2):
-            bests = [best_ref[b, pl.ds(2 * part + m, 1), :] for part in range(2)]
-            top = jnp.maximum(*bests)
-            fades = [jnp.exp2(best - top) for best in bests]
-            denom, numer = [
-                first * fades[0] + second * fades[1]
-                for first, second in (
-                    [denom_ref[b, pl.ds(2 * part + m, 1), :] for part in range(2)],
-                    [numer_ref[b, 2 * part + m] for part in range(2)],
-                )
-            ]
-            heard.append(numer / denom)
-        contrast = heard[0] - weight * heard[1]
-        contrast = contrast * lax.rsqrt(
-            jnp.mean(contrast * contrast, axis=0, keepdims=True) + epsilon
-        )
-        stacked = jnp.concatenate([contrast[:, :half], contrast[:, half:]], axis=0)
-        head_out[b] = (jnp.transpose(stacked) * gains).astype(jnp.bfloat16)
-
-        @pl.when(k > 0)
-        def _():
-            head_copy(k).start()
+        pairs = lax.div(i, 2) + 1
+        early = jnp.where(i == count - 1, count // 4, pairs)
+        lax.fori_loop(0, early, pair_of_tiles, 0)
+
+        @pl.when(i == count - 1)
+        def _():
+            @pl.loop(count // 2, count)
+            def _(n):
+                @pl.when((n < count - 1) | jnp.logical_not(lower))
+                def _():
+                    conclude(n)
+
+        lax.fori_loop(early, pairs, pair_of_tiles, 0)
+
+    @pl.when(lower)
+    def _():
+        conclude(jnp.int32(count - 1))
+
+    @pl.loop(0, count // 2)
+    def _(n):
+        conclude(count // 2 - 1 - n)
 
     held[me] = head_out[me]
-
-    @pl.loop(1, count)
-    def _(k):
-        head_copy(k).wait_recv()
-
-    for pair in range(count // 2):
+    @pl.loop(0, count // 2)
+    def _(q):
+        for k in range(2):
+            @pl.when(2 * q + k > 0)
+            def _():
+                head_copy(2 * q + k).wait_recv()
+
+        pair = flip(layer_of, q, count // 2)
         first, second = held[2 * pair], held[2 * pair + 1]
-        cut = slice(2 * pair * width, 2 * (pair + 1) * width)
         for h in range(2):
             part = slice(h * width, (h + 1) * width)
-            head_buf[0, h, :, cut] = jnp.concatenate([first[:, part], second[:, part]], axis=1)
+            span = slice(h * half, (h + 1) * half)
+            head_buf[0, q, span, :] = jnp.concatenate([first[:, part], second[:, part]], axis=1)
+        offer(head_buf, row_head + q, (q,))
+
+        @pl.when(q > 0)
+        def _():
+            pass_on(head_buf, row_head + q - 1, (q - 1,))
+
+    pass_on(head_buf, row_head + count // 2 - 1, (count // 2 - 1,))
+    loads[0].wait()
+
+    def projected(j):
+        blocks = [head_buf[j, flip(layer_of, jnp.int32(p), count // 2)] for p in range(count // 2)]
+        block = jnp.concatenate(blocks, axis=1)
+        return jnp.dot(block, proj[side[j]], preferred_element_type=f32)
+
+    total = projected(0) + projected(1) + projected(2)
+    for q in range(count // 2):
+        finish(head_buf, row_head + q, (q,))
+    total = total + projected(3)
     for h in range(2):
-        offer(head_buf, row_head + h, (h,))
-    loads[0].wait()
-    totals = [jnp.dot(head_buf[0, h], proj[col], preferred_element_type=f32) for h in range(2)]
-    for h in range(2):
-        pass_on(head_buf, row_head + h, (h,))
-    for h in range(2):
-        total = totals[h]
-        for j in (1, 2):
-            total = total + jnp.dot(head_buf[j, h], proj[side[j]], preferred_element_type=f32)
-        finish(head_buf, row_head + h, (h,))
-        total = total + jnp.dot(head_buf[3, h], proj[side[3]], preferred_element_type=f32)
         span = slice(h * half, (h + 1) * half)
-        hidden_buf[0, h] = (stream_ref[span, :].astype(f32) + total).astype(jnp.bfloat16)
+        hidden_buf[0, h] = (stream_ref[span, :].astype(f32) + total[span]).astype(jnp.bfloat16)
         offer(hidden_buf, row_hidden + h, (h,))
 
     def dispatch_far(k):
@@ -565,18 +594,23 @@
     for j in range(4):
         outgoing[j, 1] = chosen(1, j)
     dispatch_near(jnp.int32(1)).start()
-    for k in (2, 3):
-        for j in range(4):
-            outgoing[j, k] = chosen(k, j)
-        dispatch_near(jnp.int32(k)).start()
     for j in range(4):
         rows_in[j, 0] = chosen(0, j)
+    for load in loads[1:]:
+        load.wait()
+
+    def first_half(k):
+        acts[0, k] = gated_pair(scaled([rows_in[j, k] for j in range(4)]), gate, up)
+        join(acts, k, (k,)).start()
+
+    first_half(0)
     for h in range(2):
         span = slice(h * half, (h + 1) * half)
         for j, block in enumerate(scaled([hidden_buf[j, h] for j in range(4)])):
             normed[j, span, :] = block
-    for load in loads[1:]:
-        load.wait()
+    shared_buf[0] = gated_pair([normed[j] for j in range(4)], sgate, sup)
+    join(shared_buf, row_shared).start()
+    dispatch_near(jnp.int32(1)).wait_recv()
     for swap in swaps:
         swap.wait_recv()
     dispatch_far(jnp.int32(4)).wait_recv()
@@ -589,26 +623,29 @@
         later = jnp.where(p < count - 2, p + 2, p - count + 4)
         return jnp.where(p < 2, p, later)
 
-    @pl.loop(0, count + 2)
+    def second_half(buf, second, index=()):
+        return [
+            jnp.dot(buf[(0,) + index], second[c, 0], preferred_element_type=f32)
+            + jnp.dot(buf[(1,) + index], second[c, 1], preferred_element_type=f32)
+            for c in range(2)
+        ]
+
+    def scattered(k, block):
+        picked = lax.dot_general(
+            onehot[k], block, (((0,), (0,)), ((), ())), preferred_element_type=f32
+        )
+        return portions[:, k : k + 1] * picked
+
+    @pl.loop(0, count + 1)
     def _(i):
-        @pl.when((i >= 2) & (i < count - 2))
-        def _():
-            finish(rows_in, i + 2, (i + 2,))
-
-        @pl.when((i == 1) | ((i >= count - 2) & (i < count)))
-        def _():
-            dispatch_near(turn(i)).wait_recv()
-
-        @pl.when(i < count)
-        def _():
-            k = turn(i)
-            acts[0, k] = gated_pair(scaled([rows_in[j, k] for j in range(4)]), gate, up)
-            join(acts, k, (k,)).start()
-
-        @pl.when(i == 0)
-        def _():
-            shared_buf[0] = gated_pair([normed[j] for j in range(4)], sgate, sup)
-            join(shared_buf, row_shared).start()
+        @pl.when(i < 2)
+        def _():
+            for j in range(4):
+                block = hidden_buf[j].reshape(rows, cols)
+                outgoing[j, i + 2] = jnp.dot(
+                    onehot[i + 2], block, preferred_element_type=f32
+                ).astype(jnp.bfloat16)
+            dispatch_near(i + 2).start()
 
         @pl.when(i < count - 5)
         def _():
@@ -619,62 +656,71 @@
         def _():
             pass_on(rows_in, i + 4, (i + 4,))
 
-        @pl.when((i >= 1) & (i < count + 1))
-        def _():
-            k = turn(i - 1)
+        @pl.when((i >= 1) & (i < count - 3))
+        def _():
+            finish(rows_in, i + 3, (i + 3,))
+
+        @pl.when((i >= count - 3) & (i < count - 1))
+        def _():
+            dispatch_near(turn(i + 1)).wait_recv()
+
+        @pl.when(i < count - 1)
+        def _():
+            first_half(turn(i + 1))
+
+        @pl.when(i == 0)
+        def _():
+            join(acts, 0, (0,)).wait_recv()
+            for c, block in enumerate(second_half(acts, down, (0,))):
+                made_two[c] = block.astype(jnp.bfloat16)
+
+        @pl.when(i == 1)
+        def _():
+            join(shared_buf, row_shared).wait_recv()
+            for c, block in enumerate(second_half(shared_buf, sdown)):
+                shared_cols[c] = block
+
+        @pl.when((i >= 1) & (i < count))
+        def _():
+            k = turn(i)
             join(acts, k, (k,)).wait_recv()
-            own, other = [
-                jnp.dot(acts[0, k], down[c, 0], preferred_element_type=f32)
-                + jnp.dot(acts[1, k], down[c, 1], preferred_element_type=f32)
-                for c in range(2)
-            ]
+            own, other = second_half(acts, down, (k,))
             parts[0, k] = other.astype(jnp.bfloat16)
             hand_over(parts, k, (k,)).start()
             kept[k] = own
 
-        @pl.when(i == 1)
-        def _():
-            join(shared_buf, row_shared).wait_recv()
-            own, other = [
-                jnp.dot(shared_buf[0], sdown[c, 0], preferred_element_type=f32)
-                + jnp.dot(shared_buf[1], sdown[c, 1], preferred_element_type=f32)
-                for c in range(2)
-            ]
-            shared_part[0] = other.astype(jnp.bfloat16)
+        @pl.when(i == 2)
+        def _():
+            for c in range(2):
+                shared_cols[c] = shared_cols[c] + scattered(0, made_two[c])
+            shared_part[0] = shared_cols[1].astype(jnp.bfloat16)
+
+        @pl.when(i == count - 1)
+        def _():
             hand_over(shared_part, row_shared).start()
-            shared_cols[...] = own
 
         @pl.when(i >= 2)
         def _():
-            k = turn(i - 2)
+            k = turn(i - 1)
             hand_over(parts, k, (k,)).wait_recv()
             made[k] = (kept[k] + parts[1, k].astype(f32)).astype(jnp.bfloat16)
-
-            @pl.when(k > 0)
-            def _():
-                give_back(k).start()
-
+            give_back(k).start()
+
+    total = shared_cols[0]
+    for k in [1] + list(range(4, count)) + [2, 3]:
+        give_back(jnp.int32(k)).wait_recv()
+        total = total + scattered(k, back[k])
     hand_over(shared_part, row_shared).wait_recv()
-    shared_cols[...] = shared_cols[...] + shared_part[1].astype(f32)
-    back[0] = made[0]
-    for p in range(count):
-        k = p if p < 2 else (p + 2 if p < count - 2 else p - count + 4)
-        if k > 0:
-            give_back(jnp.int32(k)).wait_recv()
-        picked = lax.dot_general(
-            onehot[k], back[k], (((0,), (0,)), ((), ())), preferred_element_type=f32
-        )
-        shared_cols[...] = shared_cols[...] + portions[:, k : k + 1] * picked
+    total = total + shared_part[1].astype(f32)
     for h in range(2):
         span = slice(h * half, (h + 1) * half)
-        out_ref[span, :] = (hidden_buf[0, h].astype(f32) + shared_cols[span, :]).astype(
-            jnp.bfloat16
-        )
+        out_ref[span, :] = (hidden_buf[0, h].astype(f32) + total[span]).astype(jnp.bfloat16)
 
     for swap in swaps:
         swap.wait_send()
+    for q in range(count // 2):
+        drain(head_buf, row_head + q, (q,))
     for h in range(2):
-        drain(head_buf, row_head + h, (h,))
         drain(hidden_buf, row_hidden + h, (h,))
     join(shared_buf, row_shared).wait_send()
     hand_over(shared_part, row_shared).wait_send()
@@ -697,10 +743,10 @@
     @pl.loop(0, count)
     def _(k):
         join(acts, k, (k,)).wait_send()
-        hand_over(parts, k, (k,)).wait_send()
 
         @pl.when(k > 0)
         def _():
+            hand_over(parts, k, (k,)).wait_send()
             give_back(k).wait_send()
 
 
@@ -755,7 +801,7 @@
         + [pltpu.VMEM((2, 2, cols, cols), bf16)] * 2
         + [
             pltpu.VMEM((count, rows // 2, 2 * width), bf16),
-            pltpu.VMEM((sides, 2, rows // 2, cols), bf16),
+            pltpu.VMEM((sides, count // 2, rows, cols // (count // 2)), bf16),
             pltpu.VMEM((sides, 2, rows // 2, cols), bf16),
             pltpu.VMEM((sides, rows, cols), bf16),
             pltpu.VMEM((2, rows, cols), bf16),
@@ -768,7 +814,8 @@
             pltpu.VMEM(slots, f32),
             pltpu.VMEM(slots, bf16),
             pltpu.VMEM(slots, bf16),
-            pltpu.VMEM((rows, cols), f32),
+            pltpu.VMEM((2, capacity, cols), bf16),
+            pltpu.VMEM((2, rows, cols), f32),
             dma((9,)),
             dma((2, count)),
             dma((2, count)),
@@ -776,8 +823,8 @@
             dma((2, 2)),
             dma((count,)),
             dma((count,)),
-            dma((count + 4, 4)),
-            dma((count + 4, 4)),
+            dma((count + count // 2 + 2, 4)),
+            dma((count + count // 2 + 2, 4)),
             dma((count + 1, 2)),
             dma((count + 1, 2)),
             dma((count,)),

time: 122 us -> 118 us (0.967)
  Pallas kernels: 120 us -> 116 us
    pallas_call x1, Pallas kernels: 120 us -> 116 us  [head_per_device(): pl.pallas_call(functools.partial(layer_kernel, count, capacity, (width //...]
where the time goes in v3:
time: 118 us; the launch traced here: 117 us
  Pallas kernels  116 us (98%)
  local copies, waits for them, and re-layouts  1.67 us (1%)
    pallas_call x1, Pallas kernels, head_per_device(): pl.pallas_call(functools.partial(layer_kernel, count, capacity, (width //...  116 us

profile of v3, /device:TPU:0, one launch (start us, length us, event | category | flops | bytes accessed | tf_op | source)
XLA Modules:
  0.0 117.4 jit_solution(6074813269868358683)
XLA Ops:
  0.0 115.8 %layer.1 = bf16[256,512]{1,0:T(8,128)(2,1)} custom-call(f32[8]{0:T(128)} %lam_ref.1, bf16[256,512]{1,0:T(8,128)(2,1)} %q_ref.1, bf16[256,512]{1,0:T(8,128)(2,1)} %k_ref.1, bf16[256,512]{1,0:T(8,128)(2,1)} %v_ref.1, s32[1,256]{1,0:T(1,128)} %bitcast.22, f32[1,64]{1,0:T(1,128)} %bitcast.23, bf16[256,512]{1,0:T(8,128)(2,1)} %stream_ref.1, ...), custom_call_target="tpu_custom_call" | custom-call | tf_op jit(solution)/shard_map/layer/pallas_call | solution.py:782
  115.8 1.7 %copy.19 = bf16[256,512]{1,0:T(8,128)(2,1)} copy(bf16[256,512]{1,0:T(8,128)(2,1)} %layer.1) | data formatting | bytes 524288

commit v4 on v3

--- a/solution.py
+++ b/solution.py
@@ -608,8 +608,6 @@
         span = slice(h * half, (h + 1) * half)
         for j, block in enumerate(scaled([hidden_buf[j, h] for j in range(4)])):
             normed[j, span, :] = block
-    shared_buf[0] = gated_pair([normed[j] for j in range(4)], sgate, sup)
-    join(shared_buf, row_shared).start()
     dispatch_near(jnp.int32(1)).wait_recv()
     for swap in swaps:
         swap.wait_recv()
@@ -619,9 +617,12 @@
     def give_back(k):
         return remote(made.at[k], back.at[k], rsend.at[k], rrecv.at[k], peer(k))
 
+    far = list(range(4, count))
+    after2, after3 = count - 4 - 2, count - 4 - 1
+    sequence = [0, 1] + far[:after2] + [2] + far[after2:after3] + [3] + far[after3:]
+
     def turn(p):
-        later = jnp.where(p < count - 2, p + 2, p - count + 4)
-        return jnp.where(p < 2, p, later)
+        return sum(jnp.where(p == n, k, 0) for n, k in enumerate(sequence))
 
     def second_half(buf, second, index=()):
         return [
@@ -656,13 +657,15 @@
         def _():
             pass_on(rows_in, i + 4, (i + 4,))
 
-        @pl.when((i >= 1) & (i < count - 3))
-        def _():
-            finish(rows_in, i + 3, (i + 3,))
-
-        @pl.when((i >= count - 3) & (i < count - 1))
-        def _():
-            dispatch_near(turn(i + 1)).wait_recv()
+        coming = turn(i + 1)
+
+        @pl.when((i < count - 1) & (coming >= 4))
+        def _():
+            finish(rows_in, coming, (coming,))
+
+        @pl.when((i < count - 1) & ((coming == 2) | (coming == 3)))
+        def _():
+            dispatch_near(coming).wait_recv()
 
         @pl.when(i < count - 1)
         def _():
@@ -674,7 +677,12 @@
             for c, block in enumerate(second_half(acts, down, (0,))):
                 made_two[c] = block.astype(jnp.bfloat16)
 
-        @pl.when(i == 1)
+        @pl.when(i == 3)
+        def _():
+            shared_buf[0] = gated_pair([normed[j] for j in range(4)], sgate, sup)
+            join(shared_buf, row_shared).start()
+
+        @pl.when(i == 5)
         def _():
             join(shared_buf, row_shared).wait_recv()
             for c, block in enumerate(second_half(shared_buf, sdown)):
@@ -689,7 +697,7 @@
             hand_over(parts, k, (k,)).start()
             kept[k] = own
 
-        @pl.when(i == 2)
+        @pl.when(i == 6)
         def _():
             for c in range(2):
                 shared_cols[c] = shared_cols[c] + scattered(0, made_two[c])
@@ -707,7 +715,7 @@
             give_back(k).start()
 
     total = shared_cols[0]
-    for k in [1] + list(range(4, count)) + [2, 3]:
+    for k in sequence[1:]:
         give_back(jnp.int32(k)).wait_recv()
         total = total + scattered(k, back[k])
     hand_over(shared_part, row_shared).wait_recv()

time: 118 us -> 116 us (0.983)
  Pallas kernels: 116 us -> 113 us
    pallas_call x1, Pallas kernels: 116 us -> 113 us  [head_per_device(): pl.pallas_call(functools.partial(layer_kernel, count, capacity, (width //...]
where the time goes in v4:
time: 116 us; the launch traced here: 114 us
  Pallas kernels  113 us (97%)
  local copies, waits for them, and re-layouts  1.67 us (1%)
    pallas_call x1, Pallas kernels, head_per_device(): pl.pallas_call(functools.partial(layer_kernel, count, capacity, (width //...  113 us

profile of v4, /device:TPU:0, one launch (start us, length us, event | category | flops | bytes accessed | tf_op | source)
XLA Modules:
  0.0 114.4 jit_solution(695022371062756069)
XLA Ops:
  0.0 112.8 %layer.1 = bf16[256,512]{1,0:T(8,128)(2,1)} custom-call(f32[8]{0:T(128)} %lam_ref.1, bf16[256,512]{1,0:T(8,128)(2,1)} %q_ref.1, bf16[256,512]{1,0:T(8,128)(2,1)} %k_ref.1, bf16[256,512]{1,0:T(8,128)(2,1)} %v_ref.1, s32[1,256]{1,0:T(1,128)} %bitcast.22, f32[1,64]{1,0:T(1,128)} %bitcast.23, bf16[256,512]{1,0:T(8,128)(2,1)} %stream_ref.1, ...), custom_call_target="tpu_custom_call" | custom-call | tf_op jit(solution)/shard_map/layer/pallas_call | solution.py:790
  112.8 1.7 %copy.19 = bf16[256,512]{1,0:T(8,128)(2,1)} copy(bf16[256,512]{1,0:T(8,128)(2,1)} %layer.1) | data formatting | bytes 524288

commit v5 on v4

--- a/solution.py
+++ b/solution.py
@@ -604,13 +604,10 @@
         join(acts, k, (k,)).start()
 
     first_half(0)
-    for h in range(2):
-        span = slice(h * half, (h + 1) * half)
-        for j, block in enumerate(scaled([hidden_buf[j, h] for j in range(4)])):
-            normed[j, span, :] = block
     dispatch_near(jnp.int32(1)).wait_recv()
     for swap in swaps:
         swap.wait_recv()
+    first_half(1)
     dispatch_far(jnp.int32(4)).wait_recv()
     offer(rows_in, 4, (4,))
 
@@ -667,9 +664,9 @@
         def _():
             dispatch_near(coming).wait_recv()
 
-        @pl.when(i < count - 1)
-        def _():
-            first_half(turn(i + 1))
+        @pl.when((i >= 1) & (i < count - 1))
+        def _():
+            first_half(coming)
 
         @pl.when(i == 0)
         def _():
@@ -679,6 +676,10 @@
 
         @pl.when(i == 3)
         def _():
+            for h in range(2):
+                span = slice(h * half, (h + 1) * half)
+                for j, block in enumerate(scaled([hidden_buf[j, h] for j in range(4)])):
+                    normed[j, span, :] = block
             shared_buf[0] = gated_pair([normed[j] for j in range(4)], sgate, sup)
             join(shared_buf, row_shared).start()
 

time: 116 us -> 115 us (level)
  no operation moved by 1% of the time
where the time goes in v5:
time: 115 us; the launch traced here: 114 us
  Pallas kernels  112 us (97%)
  local copies, waits for them, and re-layouts  1.67 us (1%)
    pallas_call x1, Pallas kernels, head_per_device(): pl.pallas_call(functools.partial(layer_kernel, count, capacity, (width //...  112 us

profile of v5, /device:TPU:0, one launch (start us, length us, event | category | flops | bytes accessed | tf_op | source)
XLA Modules:
  0.0 113.6 jit_solution(16546429302755112116)
XLA Ops:
  0.0 111.9 %layer.1 = bf16[256,512]{1,0:T(8,128)(2,1)} custom-call(f32[8]{0:T(128)} %lam_ref.1, bf16[256,512]{1,0:T(8,128)(2,1)} %q_ref.1, bf16[256,512]{1,0:T(8,128)(2,1)} %k_ref.1, bf16[256,512]{1,0:T(8,128)(2,1)} %v_ref.1, s32[1,256]{1,0:T(1,128)} %bitcast.22, f32[1,64]{1,0:T(1,128)} %bitcast.23, bf16[256,512]{1,0:T(8,128)(2,1)} %stream_ref.1, ...), custom_call_target="tpu_custom_call" | custom-call | tf_op jit(solution)/shard_map/layer/pallas_call | solution.py:791
  112.0 1.7 %copy.19 = bf16[256,512]{1,0:T(8,128)(2,1)} copy(bf16[256,512]{1,0:T(8,128)(2,1)} %layer.1) | data formatting | bytes 524288
